TPU v7x, 256 devices: a whole 4x4x8 slice. The times are simulated.
256 devices in a mesh: dp: 4 (over y), kv: 32 (over z, x), tp: 2 (over core).
Axes of the slice: x: 4, y: 4, z: 8, core: 2. Of those that a mesh axis runs over, the one named last changes fastest.
Arguments:
- tokens: bfloat16 [256, 4096], P('dp', ('kv', 'tp')), may hold values from -27 to 27
- lengths: int32 [256], P(('dp', 'kv')), may hold values from 1 to 64, 4096 in all
- state: float32 [256, 4, 384, 768], P(('dp', 'kv'), 'tp'), may hold values from -6 to 6
- cache_keys: bfloat16 [256, 4, 64, 384], P(('dp', 'kv'), 'tp'), may hold values from -6 to 6
- cache_values: bfloat16 [256, 4, 64, 768], P(('dp', 'kv'), 'tp'), may hold values from -6 to 6
- cache_rates: float32 [256, 4, 64, 384], P(('dp', 'kv'), 'tp'), may hold values from 0.002 to 0.3
- attn_gain: bfloat16 [4096], P('kv'), may hold values from 0.099609375 to 1.8984375
- w_query: bfloat16 [4096, 1536], P('kv', 'tp'), may hold values from -0.09375 to 0.09375
- w_key: bfloat16 [4096, 1536], P('kv', 'tp'), may hold values from -0.09375 to 0.09375
- w_value: bfloat16 [4096, 3072], P('kv', 'tp'), may hold values from -0.09375 to 0.09375
- w_gate: bfloat16 [4096, 3072], P('kv', 'tp'), may hold values from -0.09375 to 0.09375
- w_decay: bfloat16 [4096, 1536], P('kv', 'tp'), may hold values from -0.375 to 0.375
- head_gain: bfloat16 [4, 768], P('tp'), may hold values from 0.099609375 to 1.8984375
- w_out: bfloat16 [3072, 4096], P(None, ('kv', 'tp')), may hold values from -0.109375 to 0.109375
- mlp_gain: bfloat16 [4096], replicated, may hold values from 0.099609375 to 1.8984375
- w_mlp_gate: bfloat16 [4096, 11008], P(None, ('kv', 'tp')), may hold values from -0.09375 to 0.09375
- w_mlp_up: bfloat16 [4096, 11008], P(None, ('kv', 'tp')), may hold values from -0.09375 to 0.09375
- w_mlp_down: bfloat16 [11008, 4096], P(('kv', 'tp')), may hold values from -0.15625 to 0.15625
Outputs:
- result: bfloat16 [256, 4096], P('dp', ('kv', 'tp'))
Inputs may be any that keep to these rules, and one draw needn't show every extreme that they name: `lengths`: each sequence's count of live slots in its block cache; slots from that count on take no part.
All inputs are finite; a program needn't handle non-finite values.
Results may differ from a plain program's by a relative error of at most 0.0085.
Values may be sent and summed in bfloat16 or wider, within the bound.
A program may use at most 64 MiB of HBM per device.

v0:
```python
import math

import jax
import jax.numpy as jnp
from jax import lax
from jax.sharding import PartitionSpec as P

EPS = 1e-06
GATE_NORM = 16.0
exact_mode = lax.Precision.HIGHEST


def from_everyone(array, axis):
    copies = jnp.broadcast_to(array, (lax.axis_size(axis), *array.shape))
    return lax.all_to_all(copies, axis, split_axis=0, concat_axis=0, tiled=True)


def joined_along(parts, dim):
    lengths = list(parts.shape[1:])
    lengths[dim] *= parts.shape[0]
    return jnp.moveaxis(parts, 0, dim).reshape(lengths)


def gathered_copies(array, axis, dim):
    parts = from_everyone(array, axis)
    return joined_along(parts, dim)


def cut_along(array, dim, size):
    before, after = (array.shape[:dim], array.shape[dim + 1 :])
    return jnp.moveaxis(array.reshape(*before, size, -1, *after), dim, 0)


def sum_at_owner(array, axis, dim):
    size = lax.axis_size(axis)
    parts = lax.all_to_all(cut_along(array, dim, size), axis, 0, 0, tiled=True)
    return jnp.sum(parts.astype(jnp.float32), axis=0)


def side_by_side(arrays, axis, dim, along):
    widths = [math.prod(a.shape[along:]) for a in arrays]
    both = jnp.concatenate(
        [a.reshape(*a.shape[:along], w) for a, w in zip(arrays, widths)], axis=along
    )
    out = sum_at_owner(both, axis, dim)
    parts = jnp.split(out, [sum(widths[:k]) for k in range(1, len(widths))], axis=along)
    return tuple((b.reshape(*out.shape[:along], *a.shape[along:]) for a, b in zip(arrays, parts)))


def front_part(query, key_new, log_decay, state, cache_keys, cache_rates, lengths):
    span = cache_keys.shape[2]
    live = (jnp.arange(span, dtype=jnp.int32)[None, :] < lengths[:, None]).astype(jnp.float32)
    running = jnp.cumsum(cache_rates * live[:, None, :, None], axis=2)
    total = running[:, :, -1:, :]
    weight = jnp.exp(running - total + log_decay[:, :, None, :])
    scores = (
        jnp.einsum(
            "bhd,bhjd->bhj", query, weight * cache_keys.astype(jnp.float32), precision=exact_mode
        )
        * live[:, None, :]
    )
    carried = jnp.einsum(
        "bhd,bhde->bhe", query * jnp.exp(log_decay - total[:, :, 0, :]), state, precision=exact_mode
    )
    own = jnp.sum(query * key_new, axis=-1, keepdims=True)
    return (scores, carried, own)


def back_part(scores, carried, own, value_new, cache_values, gate, head_gain):
    inner = jnp.einsum(
        "bhj,bhje->bhe", scores, cache_values.astype(jnp.float32), precision=exact_mode
    )
    attended = carried + inner + own * value_new
    normed = attended * lax.rsqrt(jnp.mean(attended * attended, axis=-1, keepdims=True) + EPS)
    normed = normed * head_gain.astype(jnp.float32)
    return (jax.nn.silu(gate) * normed).astype(jnp.bfloat16)


def open_heads(
    query_sum, key_sum, decay_sum, own_squares, width, state, cache_keys, cache_rates, lengths
):
    seq_dev, heads_dev, key_dim = (state.shape[0], state.shape[1], state.shape[2])
    inv_rms = lax.rsqrt(own_squares / width + EPS)[:, None]
    query = (query_sum * inv_rms * key_dim ** (-0.5)).reshape(seq_dev, heads_dev, key_dim)
    key_new = (key_sum * inv_rms).reshape(seq_dev, heads_dev, key_dim)
    log_decay = (jax.nn.log_sigmoid(decay_sum * inv_rms) / GATE_NORM).reshape(
        seq_dev, heads_dev, key_dim
    )
    scores, carried, own = front_part(
        query, key_new, log_decay, state, cache_keys, cache_rates, lengths
    )
    return (inv_rms, scores, carried, own)


def close_heads(opened, value_sum, gate_sum, cache_values, head_gain):
    inv_rms, scores, carried, own = opened
    seq_dev, heads_dev, value_dim = carried.shape
    value_new = (value_sum * inv_rms).reshape(seq_dev, heads_dev, value_dim)
    gate = (gate_sum * inv_rms).reshape(seq_dev, heads_dev, value_dim)
    heads = back_part(scores, carried, own, value_new, cache_values, gate, head_gain)
    return heads.reshape(seq_dev, heads_dev * value_dim)


def shards(
    tokens,
    lengths,
    state,
    cache_keys,
    cache_values,
    cache_rates,
    attn_gain,
    w_query,
    w_key,
    w_value,
    w_gate,
    w_decay,
    head_gain,
    w_out,
    mlp_gain,
    w_mlp_gate,
    w_mlp_up,
    w_mlp_down,
):
    seq_dev, heads_dev, value_dim = (state.shape[0], state.shape[1], state.shape[3])
    width = mlp_gain.shape[0]
    n_kv = lax.axis_size("kv")
    n_tp = lax.axis_size("tp")
    block = gathered_copies(tokens, "tp", 1).astype(jnp.float32)
    squares = jnp.sum(block * block, axis=1)
    scaled = (block * attn_gain.astype(jnp.float32)).astype(jnp.bfloat16)
    query_part = jnp.dot(scaled, w_query, preferred_element_type=jnp.float32)
    key_part = jnp.dot(scaled, w_key, preferred_element_type=jnp.float32)
    decay_part = jnp.dot(scaled, w_decay, preferred_element_type=jnp.float32)
    value_part = jnp.dot(scaled, w_value, preferred_element_type=jnp.float32)
    gate_part = jnp.dot(scaled, w_gate, preferred_element_type=jnp.float32)
    query_sum, key_sum, decay_sum, value_sum, gate_sum, own_squares = side_by_side(
        (
            query_part.astype(jnp.bfloat16),
            key_part.astype(jnp.bfloat16),
            decay_part.astype(jnp.bfloat16),
            value_part.astype(jnp.bfloat16),
            gate_part.astype(jnp.bfloat16),
            squares.astype(jnp.bfloat16),
        ),
        "kv",
        0,
        1,
    )
    opened = open_heads(
        query_sum, key_sum, decay_sum, own_squares, width, state, cache_keys, cache_rates, lengths
    )
    heads = close_heads(opened, value_sum, gate_sum, cache_values, head_gain)
    columns = w_out.shape[1]
    stacked = w_out.reshape(n_tp, heads_dev * value_dim, columns)
    piece = gathered_copies(heads.reshape(1, seq_dev, heads_dev * value_dim), ("kv", "tp"), 0)
    terms = jnp.einsum("psk,tkc->ptsc", piece, stacked, preferred_element_type=jnp.float32)
    owner = jnp.arange(piece.shape[0], dtype=jnp.int32)
    row_match = (owner // n_tp)[:, None, None] == jnp.arange(n_kv, dtype=jnp.int32)[None, :, None]
    head_match = (owner % n_tp)[:, None, None] == jnp.arange(n_tp, dtype=jnp.int32)[None, None, :]
    chosen = (row_match & head_match).astype(jnp.float32)
    projected = jnp.einsum("prt,ptsc->rsc", chosen, terms, precision=exact_mode)
    projected = projected.reshape(n_kv * seq_dev, columns)
    after = (tokens.astype(jnp.float32) + projected).astype(jnp.bfloat16)
    whole = gathered_copies(after, ("kv", "tp"), 1).astype(jnp.float32)
    inv_second = lax.rsqrt(jnp.mean(whole * whole, axis=1, keepdims=True) + EPS)
    normed = (whole * inv_second * mlp_gain.astype(jnp.float32)).astype(jnp.bfloat16)
    gate_ff = jnp.dot(normed, w_mlp_gate, preferred_element_type=jnp.float32)
    up_ff = jnp.dot(normed, w_mlp_up, preferred_element_type=jnp.float32)
    hidden = (jax.nn.silu(gate_ff) * up_ff).astype(jnp.bfloat16)
    terms = jnp.dot(hidden, w_mlp_down, preferred_element_type=jnp.float32)
    own_share = sum_at_owner(terms.astype(jnp.bfloat16), ("kv", "tp"), 1)
    return (after.astype(jnp.float32) + own_share).astype(jnp.bfloat16)


def solution(mesh):
    placed = (
        P("dp", ("kv", "tp")),
        P(("dp", "kv")),
        P(("dp", "kv"), "tp", None, None),
        P(("dp", "kv"), "tp", None, None),
        P(("dp", "kv"), "tp", None, None),
        P(("dp", "kv"), "tp", None, None),
        P("kv"),
        P("kv", "tp"),
        P("kv", "tp"),
        P("kv", "tp"),
        P("kv", "tp"),
        P("kv", "tp"),
        P("tp", None),
        P(None, ("kv", "tp")),
        P(),
        P(None, ("kv", "tp")),
        P(None, ("kv", "tp")),
        P(("kv", "tp"), None),
    )
    return jax.shard_map(
        shards, mesh=mesh, in_specs=placed, out_specs=P("dp", ("kv", "tp")), check_vma=False
    )
```

profile of v0, /device:TPU:1, one launch (start us, length us, event | category | flops | bytes accessed | tf_op | source)
XLA Modules:
  0.0 139.8 jit_solution(18437428278168510503)
XLA Ops:
  0.0 0.9 broadcast_in_dim.6
  1.0 6.6 %all_to_all.25 = bf16[2,2,2048]{2,1,0:T(2,128)(2,1)S(1)} all-to-all(bf16[2,2,2048]{2,1,0:T(2,128)(2,1)S(1)} %reshape.206), channel_id=1, replica_groups=mesh['dp'=4,'kv'=32,'tp'=2] {'tp'}, dimensions={0} | all-to-all | bytes 32768 | tf_op jit(solution)/shard_map/all_to_all | solution.py:15
  7.8 0.7 convert_element_type.117
  8.8 1.1 convolution_convert_fusion.3
  10.0 1.1 convolution_convert_fusion.4
  12.0 0.7 constant_dynamic-update-slice_fusion.5
  12.7 0.7 constant_dynamic-update-slice_fusion.4
  13.4 0.8 constant_dynamic-update-slice_fusion.3
  14.2 0.8 constant_dynamic-update-slice_fusion.2
  15.0 0.8 constant_dynamic-update-slice_fusion.1
  15.8 0.6 constant_dynamic-update-slice_fusion
  16.5 9.3 %all-to-all-start.1 = ((bf16[32,2,5377]{2,1,0:T(2,128)(2,1)}), bf16[32,2,5377]{2,1,0:T(2,128)(2,1)S(1)}, u32[]{:S(2)}, u32[]{:S(2)}) async-start(bf16[32,2,5377]{2,1,0:T(2,128)(2,1)} %constant_dynamic-update-slice_fusion), calls=%async_computation.1 | async-start | bytes 1409024 | tf_op jit(solution)/shard_map/all_to_all | solution.py:36
  26.4 19.4 %all-to-all-done.1 = bf16[32,2,5377]{2,1,0:T(2,128)(2,1)S(1)} async-done(((bf16[32,2,5377]{2,1,0:T(2,128)(2,1)}), bf16[32,2,5377]{2,1,0:T(2,128)(2,1)S(1)}, u32[]{:S(2)}, u32[]{:S(2)}) %all-to-all-start.1) | async-done | bytes 688288 | tf_op jit(solution)/shard_map/all_to_all | solution.py:36
  45.9 0.6 convert_reduce_fusion.1
  47.6 4.7 %fusion.31 = f32[2,2,1,768]{3,2,1,0:T(1,128)S(1)} fusion(f32[2,2,384,768]{3,2,1,0:T(8,128)} %param.20, f32[2,2,384,1]{2,1,0,3:T(2,128)S(1)} %get-tuple-element.12), kind=kOutput, calls=%fused_computation.70 | convolution fusion | flops 14155776 | bytes 4737024 | tf_op jit(solution)/shard_map/bhd,bhde->bhe/dot_general | solution.py:62
  52.8 0.9 broadcast_in_dim.7
  53.8 7.3 %all-to-all-start.2 = ((bf16[64,1,2,1536]{3,2,1,0:T(2,128)(2,1)}), bf16[64,1,2,1536]{3,2,1,0:T(2,128)(2,1)S(1)}, u32[]{:S(2)}, u32[]{:S(2)}) async-start(bf16[64,1,2,1536]{3,2,1,0:T(2,128)(2,1)} %broadcast_in_dim.7), calls=%async_computation.2 | async-start | bytes 786432 | tf_op jit(solution)/shard_map/all_to_all | solution.py:15
  61.2 15.1 %all-to-all-done.2 = bf16[64,1,2,1536]{3,2,1,0:T(2,128)(2,1)S(1)} async-done(((bf16[64,1,2,1536]{3,2,1,0:T(2,128)(2,1)}), bf16[64,1,2,1536]{3,2,1,0:T(2,128)(2,1)S(1)}, u32[]{:S(2)}, u32[]{:S(2)}) %all-to-all-start.2) | async-done | bytes 393248 | tf_op jit(solution)/shard_map/all_to_all | solution.py:15
  77.2 1.5 %reshape.208 = bf16[64,2,2048]{2,1,0:T(2,128)(2,1)} reshape(bf16[64,64,64]{2,1,0:T(8,128)(2,1)S(1)} %broadcast_in_dim.8) | data formatting | bytes 1048576
  78.7 5.5 %all-to-all-start.3 = ((bf16[64,2,2048]{2,1,0:T(2,128)(2,1)}), bf16[64,2,2048]{2,1,0:T(2,128)(2,1)S(1)}, u32[]{:S(2)}, u32[]{:S(2)}) async-start(bf16[64,2,2048]{2,1,0:T(2,128)(2,1)} %reshape.208), calls=%async_computation.3 | async-start | bytes 1048576 | tf_op jit(solution)/shard_map/all_to_all | solution.py:15
  84.2 17.7 %all-to-all-done.3 = bf16[64,2,2048]{2,1,0:T(2,128)(2,1)S(1)} async-done(((bf16[64,2,2048]{2,1,0:T(2,128)(2,1)}), bf16[64,2,2048]{2,1,0:T(2,128)(2,1)S(1)}, u32[]{:S(2)}, u32[]{:S(2)}) %all-to-all-start.3) | async-done | bytes 524320 | tf_op jit(solution)/shard_map/all_to_all | solution.py:15
  101.9 0.7 reshape.209
  103.2 2.6 %copy.47 = f32[64,64,64]{2,1,0:T(8,128)} copy(f32[64,64,64]{2,0,1:T(8,128)S(1)} %convert_bitcast_fusion) | data formatting | bytes 2097152 | tf_op jit(solution)/shard_map/convert_element_type | solution.py:164
  105.8 2.1 %reshape.192 = f32[64,4096]{1,0:T(8,128)S(1)} reshape(f32[64,64,64]{2,1,0:T(8,128)} %copy.47) | data formatting | bytes 2097152 | tf_op jit(solution)/shard_map/convert_element_type | solution.py:164
  107.9 2.0 %fusion.38 = f32[64,172]{1,0:T(8,128)S(1)} fusion(bf16[4096,172]{0,1:T(8,128)(2,1)} %param.33, f32[64,4096]{1,0:T(8,128)S(1)} %reshape.192, f32[4096]{0:T(1024)S(1)} %convert_element_type.138, f32[64]{0:T(128)S(1)} %add_rsqrt_fusion.1), kind=kOutput, calls=%fused_computation.90 | convolution fusion | flops 90963968 | bytes 2518272 | tf_op jit(solution)/shard_map/dot_general | solution.py:167
  109.9 2.6 %convolution_convert_fusion = bf16[64,4096]{1,0:T(8,128)(2,1)S(1)} fusion(bf16[172,4096]{1,0:T(8,128)(2,1)S(1)} %copy-done, bf16[4096,172]{0,1:T(8,128)(2,1)} %param.34, f32[64,172]{1,0:T(8,128)S(1)} %fusion.38, f32[64,4096]{1,0:T(8,128)S(1)} %reshape.192, f32[4096]{0:T(1024)S(1)} %convert_element_type.138, f32[64]{0:T(128)S(1)} %add_rsqrt_fusion.1), kind=kOutput, calls=%fused_computation | convolution fusion | flops 181469696 | bytes 4451584 | tf_op jit(solution)/shard_map/dot_general | solution.py:170
  112.5 1.1 reshape.190
  113.6 0.7 copy.78
  114.3 0.7 reshape.210
  115.1 23.2 %all_to_all.26 = bf16[64,2,2048]{2,1,0:T(2,128)(2,1)S(1)} all-to-all(bf16[64,2,2048]{2,1,0:T(2,128)(2,1)S(1)} %reshape.210), channel_id=1, replica_groups=mesh['dp'=4,'kv'=32,'tp'=2] {'kv','tp'}, dimensions={0} | all-to-all | bytes 1048576 | tf_op jit(solution)/shard_map/all_to_all | solution.py:36
  138.3 0.7 reshape.211
  139.2 0.6 add_convert_fusion
  (77 shorter events, 5.4 us)
Async XLA Ops:
  0.0 109.9 %copy-start = (bf16[172,4096]{1,0:T(8,128)(2,1)S(1)}, bf16[172,4096]{1,0:T(8,128)(2,1)}, u32[]{:S(2)}) copy-start(bf16[172,4096]{1,0:T(8,128)(2,1)} %param.35) | copy-start | bytes 4227076
  0.0 11.1 %copy-start.5 = (bf16[128,768]{1,0:T(8,128)(2,1)S(1)}, bf16[128,768]{1,0:T(8,128)(2,1)}, u32[]{:S(2)}) copy-start(bf16[128,768]{1,0:T(8,128)(2,1)} %param.25) | copy-start | bytes 589828
  0.0 11.3 %copy-start.1 = (bf16[128,1536]{1,0:T(8,128)(2,1)S(1)}, bf16[128,1536]{1,0:T(8,128)(2,1)}, u32[]{:S(2)}) copy-start(bf16[128,1536]{1,0:T(8,128)(2,1)} %param.28) | copy-start | bytes 1179652
  7.8 3.9 %copy-start.2 = (bf16[128,1536]{1,0:T(8,128)(2,1)S(1)}, bf16[128,1536]{1,0:T(8,128)(2,1)}, u32[]{:S(2)}) copy-start(bf16[128,1536]{1,0:T(8,128)(2,1)} %param.27) | copy-start | bytes 1179652
  11.9 13.9 %copy-start.9 = (bf16[2,768]{1,0:T(2,128)(2,1)S(1)}, bf16[2,768]{1,0:T(2,128)(2,1)}, u32[]{:S(2)}) copy-start(bf16[2,768]{1,0:T(2,128)(2,1)} %param.30) | copy-start | bytes 9220
  11.9 13.9 %copy-start.11 = (s32[2]{0:T(128)S(1)}, s32[2]{0:T(128)}, u32[]{:S(2)}) copy-start(s32[2]{0:T(128)} %param.19) | copy-start | bytes 28
  12.0 14.0 %copy-start.3 = (f32[2,2,64,384]{3,2,1,0:T(8,128)S(1)}, f32[2,2,64,384]{3,2,1,0:T(8,128)}, u32[]{:S(2)}) copy-start(f32[2,2,64,384]{3,2,1,0:T(8,128)} %param.23) | copy-start | bytes 1179652
  16.5 29.4 %all-to-all-start.1 = ((bf16[32,2,5377]{2,1,0:T(2,128)(2,1)}), bf16[32,2,5377]{2,1,0:T(2,128)(2,1)S(1)}, u32[]{:S(2)}, u32[]{:S(2)}) async-start(bf16[32,2,5377]{2,1,0:T(2,128)(2,1)} %constant_dynamic-update-slice_fusion), calls=%async_computation.1 | async-start | bytes 1409024 | tf_op jit(solution)/shard_map/all_to_all | solution.py:36
  25.8 21.0 %copy-start.6 = (bf16[2,2,64,384]{3,2,1,0:T(8,128)(2,1)S(1)}, bf16[2,2,64,384]{3,2,1,0:T(8,128)(2,1)}, u32[]{:S(2)}) copy-start(bf16[2,2,64,384]{3,2,1,0:T(8,128)(2,1)} %param.21) | copy-start | bytes 589828
  47.6 4.7 %copy-start.4 = (bf16[2,2,64,768]{3,2,1,0:T(8,128)(2,1)S(1)}, bf16[2,2,64,768]{3,2,1,0:T(8,128)(2,1)}, u32[]{:S(2)}) copy-start(bf16[2,2,64,768]{3,2,1,0:T(8,128)(2,1)} %param.22) | copy-start | bytes 1179652
  52.3 24.0 %copy-start.10 = (bf16[3072,64]{0,1:T(8,128)(2,1)S(1)}, bf16[3072,64]{0,1:T(8,128)(2,1)}, u32[]{:S(2)}) copy-start(bf16[3072,64]{0,1:T(8,128)(2,1)} %param.31) | copy-start | bytes 1179652
  52.5 24.4 %copy-start.7 = (bf16[64,64]{1,0:T(8,128)(2,1)S(1)}, bf16[64,64]{1,0:T(8,128)(2,1)}, u32[]{:S(2)}) copy-start(bf16[64,64]{1,0:T(8,128)(2,1)} %param.18) | copy-start | bytes 24580
  53.8 22.5 %all-to-all-start.2 = ((bf16[64,1,2,1536]{3,2,1,0:T(2,128)(2,1)}), bf16[64,1,2,1536]{3,2,1,0:T(2,128)(2,1)S(1)}, u32[]{:S(2)}, u32[]{:S(2)}) async-start(bf16[64,1,2,1536]{3,2,1,0:T(2,128)(2,1)} %broadcast_in_dim.7), calls=%async_computation.2 | async-start | bytes 786432 | tf_op jit(solution)/shard_map/all_to_all | solution.py:15
  77.2 7.0 %copy-start.8 = (bf16[4096]{0:T(1024)(128)(2,1)S(1)}, bf16[4096]{0:T(1024)(128)(2,1)}, u32[]{:S(2)}) copy-start(bf16[4096]{0:T(1024)(128)(2,1)} %param.32) | copy-start | bytes 24580
  78.7 23.1 %all-to-all-start.3 = ((bf16[64,2,2048]{2,1,0:T(2,128)(2,1)}), bf16[64,2,2048]{2,1,0:T(2,128)(2,1)S(1)}, u32[]{:S(2)}, u32[]{:S(2)}) async-start(bf16[64,2,2048]{2,1,0:T(2,128)(2,1)} %reshape.208), calls=%async_computation.3 | async-start | bytes 1048576 | tf_op jit(solution)/shard_map/all_to_all | solution.py:15
where the time goes:
time: 140 us
  waiting for transfers between devices  52.2 us (37%)
  blocking collectives  29.8 us (21%)
  starting transfers between devices  22.1 us (16%)
  local copies, waits for them, and re-layouts  17.7 us (13%)
  matrix products  13.4 us (10%)
  other arithmetic  4.14 us (3%)
    all_to_all x2, waiting for transfers between devices, from_everyone(): return lax.all_to_all(copies, axis, split_axis=0, concat_axis=0, tiled=True)  32.8 us
    all_to_all x1, blocking collectives, sum_at_owner(): parts = lax.all_to_all(cut_along(array, dim, size), axis, 0, 0, tiled=True)  23.2 us
    all_to_all x1, waiting for transfers between devices, sum_at_owner(): parts = lax.all_to_all(cut_along(array, dim, size), axis, 0, 0, tiled=True)  19.4 us
    all_to_all x2, starting transfers between devices, from_everyone(): return lax.all_to_all(copies, axis, split_axis=0, concat_axis=0, tiled=True)  12.8 us
    all_to_all x1, starting transfers between devices, sum_at_owner(): parts = lax.all_to_all(cut_along(array, dim, size), axis, 0, 0, tiled=True)  9.33 us
    unnamed x37, local copies, waits for them, and re-layouts  7.74 us
    all_to_all x1, blocking collectives, from_everyone(): return lax.all_to_all(copies, axis, split_axis=0, concat_axis=0, tiled=True)  6.57 us
    dot_general x1, matrix products, front_part(): jnp.einsum('bhd,bhde->bhe', query * jnp.exp(log_decay - total[:, :, 0, :]...  4.71 us
  transfers between devices with their start and end apart: 3, of which 3 were waited for; matrix products, arithmetic and copies ran while one was open for 0% of the time, Pallas kernels for 0%

commit v1 on v0

v1 whole, which is shorter than its diff:
```python
import functools

import jax
import jax.numpy as jnp
from jax import lax
from jax.experimental import pallas as pl
from jax.experimental.pallas import tpu as pltpu
from jax.sharding import PartitionSpec as P

EPS = 1e-06
GATE_NORM = 16.0
NX = 4
LANES = 128
MESH = pl.DeviceIdType.MESH
F32 = jnp.float32
BF16 = jnp.bfloat16


def dot(a, b, dims=((1,), (0,))):
    return lax.dot_general(a, b, (dims, ((), ())), preferred_element_type=F32)


def high_low(a):
    high = a.astype(BF16)
    return high, (a - high.astype(F32)).astype(BF16)


def kernel(
    sizes,
    tokens,
    lengths,
    state,
    cache_keys,
    cache_values,
    cache_rates,
    attn_gain,
    w_query,
    w_key,
    w_value,
    w_gate,
    w_decay,
    head_gain,
    w_out,
    mlp_gain,
    w_mlp_gate,
    w_mlp_up,
    w_mlp_down,
    out,
    tok,
    tokf,
    wq,
    wk,
    wd,
    wv,
    wg,
    st,
    ck,
    cv,
    cr,
    wo,
    wmg,
    wmu,
    wmd,
    x0,
    x1,
    ra0,
    ra1,
    rs0,
    rs1,
    rb0,
    rb1,
    zf,
    zs0,
    zs1,
    zr0,
    zr1,
    memory,
    pack0,
    pack1,
    qe,
    att,
    hg,
    headf,
    headb,
    headsf,
    lhs,
    whole,
    hidden,
    dpart,
    dpeer,
    dx,
    dra,
    drs,
    drb,
    dzs,
    dzr,
    outf,
    lsem,
    psem,
    xsem,
    zsem,
    hz,
    hx,
    hp,
    hr,
    az,
    ax,
    ap,
    ar,
    dsem,
    dzsem,
):
    nz, qb, vb, dk, width = sizes
    rows2 = 2 * nz
    kv = lax.axis_index("kv")
    c = lax.axis_index("tp")
    other = 1 - c
    z = kv // NX
    x = kv % NX
    xr = (x + 1) % NX
    xl = (x + NX - 1) % NX
    xo = (x + 2) % NX
    steps = [((d + 1) // 2) * (1 if d % 2 else -1) for d in range(1, nz)]
    far = [(z + (s % nz)) % nz for s in steps][::-1]
    near = [(z + (s % nz)) % nz for s in steps]
    sides = [(x + d) % NX for d in (2, 1, 3)]

    def local(i, src, dst):
        copy = pltpu.make_async_copy(src, dst, lsem.at[i])
        copy.start()
        return copy

    def remote(src, dst, send, recv, to_kv, to_tp):
        return pltpu.make_async_remote_copy(
            src_ref=src,
            dst_ref=dst,
            send_sem=send,
            recv_sem=recv,
            device_id={"kv": to_kv, "tp": to_tp},
            device_id_type=MESH,
        )

    sent = []

    def send(*args):
        copy = remote(*args)
        copy.start()
        sent.append(copy)

    in_tok = local(0, tokens, tok.at[c])
    in_w = [
        local(1 + i, src, dst)
        for i, (src, dst) in enumerate(
            ((w_query, wq), (w_key, wk), (w_decay, wd), (w_value, wv), (w_gate, wg))
        )
    ]
    in_cache = [
        local(6 + i, src, dst)
        for i, (src, dst) in enumerate(((cache_rates, cr), (cache_keys, ck), (cache_values, cv)))
    ]
    in_state = local(9, state, st)
    in_out = local(10, w_out, wo.at[c])
    in_mlp = [
        local(11 + i, src, dst)
        for i, (src, dst) in enumerate(((w_mlp_gate, wmg), (w_mlp_up, wmu), (w_mlp_down, wmd)))
    ]

    barrier = pltpu.get_barrier_semaphore()

    def greet(to_kv, to_tp):
        pl.semaphore_signal(
            barrier, inc=1, device_id={"kv": to_kv, "tp": to_tp}, device_id_type=MESH
        )

    for zp in far:
        greet(zp * NX + x, c)
        greet(zp * NX + x, other)
    for xp in sides:
        greet(z * NX + xp, c)
    greet(kv, other)
    zf[...] = jnp.zeros_like(zf)
    for h in range(2):
        for b in range(vb // 2):
            hg[h * (vb // 2) + b : h * (vb // 2) + b + 1, :] = head_gain[
                h : h + 1, b * LANES : (b + 1) * LANES
            ].astype(F32)
    pl.semaphore_wait(barrier, 2 * len(far) + len(sides) + 1)

    in_tok.wait()
    send(tok.at[c], tok.at[c], psem.at[0], psem.at[1], kv, other)
    in_out.wait()
    send(wo.at[c], wo.at[c], psem.at[2], psem.at[3], kv, other)
    remote(tok.at[other], tok.at[other], psem.at[0], psem.at[1], kv, other).wait_recv()
    tokf[...] = jnp.concatenate([tok[0].astype(F32), tok[1].astype(F32)], axis=1)
    block = jnp.concatenate(
        [
            tokf[pl.ds(2 * xp + i, nz, stride=2 * NX), :]
            for xp in range(NX)
            for i in range(2)
        ],
        axis=0,
    )
    squares = jnp.sum(block * block, axis=1, keepdims=True)
    scaled = (block * attn_gain[...].astype(F32)).astype(BF16)

    def put(target, b, values):
        half = target.shape[3] // LANES
        at = (b % half) * LANES
        for xp in range(NX):
            target[xp, b // half, :, at : at + LANES] = values[
                xp * rows2 : (xp + 1) * rows2
            ].astype(BF16)

    def project(copy, weight, target, start):
        copy.wait()
        part = dot(scaled, weight[...])
        for b in range(weight.shape[1] // LANES):
            put(target, start + b, part[:, b * LANES : (b + 1) * LANES])

    def x_first(src, first, back, sems, base):
        send(src.at[xo, 0], first.at[0], sems.at[0, base], sems.at[1, base], z * NX + xr, c)
        send(src.at[xo, 1], first.at[1], sems.at[0, base + 1], sems.at[1, base + 1], z * NX + xl, c)
        send(src.at[xr, 1], back.at[0, 1], sems.at[0, base + 2], sems.at[1, base + 2], z * NX + xr, c)
        send(src.at[xl, 0], back.at[1, 0], sems.at[0, base + 3], sems.at[1, base + 3], z * NX + xl, c)

    def x_second(src, first, relay, back, sems, base):
        remote(
            first.at[0], first.at[0], sems.at[0, base], sems.at[1, base], z * NX + xl, c
        ).wait_recv()
        relay[0] = (src[xr, 0].astype(F32) + first[0].astype(F32)).astype(BF16)
        send(relay.at[0], back.at[0, 0], sems.at[0, base + 4], sems.at[1, base + 4], z * NX + xr, c)
        remote(
            first.at[1], first.at[1], sems.at[0, base + 1], sems.at[1, base + 1], z * NX + xr, c
        ).wait_recv()
        relay[1] = (src[xl, 1].astype(F32) + first[1].astype(F32)).astype(BF16)
        send(relay.at[1], back.at[1, 1], sems.at[0, base + 5], sems.at[1, base + 5], z * NX + xl, c)

    def x_wait(back, sems, base, side, half):
        slot = {(0, 1): 2, (1, 0): 3, (0, 0): 4, (1, 1): 5}[(side, half)]
        remote(
            back.at[side, half],
            back.at[side, half],
            sems.at[0, base + slot],
            sems.at[1, base + slot],
            z * NX + (xr if side else xl),
            c,
        ).wait_recv()

    def x_sum(src, back, half):
        return src[x, half].astype(F32) + back[0, half].astype(F32) + back[1, half].astype(F32)

    project(in_w[0], wq, x0, 0)
    project(in_w[1], wk, x0, qb)
    project(in_w[2], wd, x0, 2 * qb)
    put(x0, 3 * qb, jnp.broadcast_to(squares, (squares.shape[0], LANES)))
    for b in range(3 * qb + 1, 2 * (x0.shape[3] // LANES)):
        put(x0, b, jnp.zeros((squares.shape[0], LANES), F32))
    x_first(x0, ra0, rb0, xsem, 0)
    project(in_w[3], wv, x1, 0)
    project(in_w[4], wg, x1, vb)
    x_first(x1, ra1, rb1, xsem, 6)

    span = ck.shape[2]
    hb = vb // 2
    later = (
        lax.broadcasted_iota(jnp.int32, (span, span), 1)
        > lax.broadcasted_iota(jnp.int32, (span, span), 0)
    ).astype(BF16)
    ones = jnp.ones((span, LANES), BF16)
    slots = lax.broadcasted_iota(jnp.int32, (span, 1), 0)

    def fold(i, h):
        live = (slots < lengths[i]).astype(F32)
        rates = cr[i, h] * live
        high, low = high_low(rates)
        rest = dot(later, high) + dot(later, low)
        keys = jnp.exp(-rest) * ck[i, h].astype(F32) * live
        shrink = jnp.exp(-(dot(high, ones, ((0,), (0,))) + dot(low, ones, ((0,), (0,)))))
        high, low = high_low(keys)
        value = cv[i, h]
        inner = dot(high, value, ((0,), (0,))) + dot(low, value, ((0,), (0,)))
        for b in range(hb):
            cols = slice(b * LANES, (b + 1) * LANES)
            memory[i, h, :, cols] = (st[i, h, :, cols] * shrink + inner[:, cols]).astype(BF16)

    for copy in in_cache:
        copy.wait()
    in_state.wait()
    x_second(x0, ra0, rs0, rb0, xsem, 0)
    x_second(x1, ra1, rs1, rb1, xsem, 6)

    slots_row = zf.shape[0] // rows2

    def z_send(src, back, packed, landing, base, sem_base):
        half = src.shape[3] // LANES
        for hh, side in ((1, 0), (0, 1), (0, 0), (1, 1)):
            x_wait(back, xsem, base, side, hh)
        for hh in (0, 1):
            total = x_sum(src, back, hh)
            for b in range(half):
                for i in range(2):
                    zf[pl.ds(i * slots_row + hh * half + b, nz, stride=2 * slots_row), :] = total[
                        i * nz : (i + 1) * nz, b * LANES : (b + 1) * LANES
                    ]
        for zp in range(nz):
            packed[zp] = zf[zp * 2 * slots_row : (zp + 1) * 2 * slots_row, :].astype(BF16)
        for k, zp in enumerate(far):
            send(
                packed.at[zp],
                landing.at[z],
                zsem.at[0, sem_base + k],
                zsem.at[1, sem_base + z],
                zp * NX + x,
                c,
            )

    def z_sum(packed, landing, sem_base):
        for zp in near:
            remote(
                landing.at[zp],
                landing.at[zp],
                zsem.at[0, sem_base],
                zsem.at[1, sem_base + zp],
                zp * NX + x,
                c,
            ).wait_recv()
        total = packed[z].astype(F32)
        for zp in near:
            total = total + landing[zp].astype(F32)
        return total

    z_send(x0, rb0, zs0, zr0, 0, 0)
    z_send(x1, rb1, zs1, zr1, 6, nz)
    for i in range(2):
        for h in range(2):
            fold(i, h)

    pack0[...] = z_sum(zs0, zr0, 0)
    own = []
    inverse = []
    qh = qb // 2
    for i in range(2):
        at = i * slots_row
        inv = lax.rsqrt(pack0[at + 3 * qb : at + 3 * qb + 1, :] * (1.0 / width) + EPS)
        inverse.append(inv)
        query = pack0[at : at + qb, :] * inv * dk ** (-0.5)
        key = pack0[at + qb : at + 2 * qb, :] * inv
        raw = pack0[at + 2 * qb : at + 3 * qb, :] * inv
        decay = (jnp.minimum(raw, 0.0) - jnp.log1p(jnp.exp(-jnp.abs(raw)))) / GATE_NORM
        qe[i * qb : (i + 1) * qb, :] = query * jnp.exp(decay)
        both = query * key
        for h in range(2):
            part = jnp.sum(both[h * qh : (h + 1) * qh, :], axis=0, keepdims=True)
            own.append(jnp.sum(part, axis=1, keepdims=True))
    for i in range(2):
        for h in range(2):
            row = jnp.concatenate(
                [qe[i * qb + h * qh + b : i * qb + h * qh + b + 1, :] for b in range(qh)], axis=1
            )
            high, low = high_low(row)
            got = dot(jnp.concatenate([high, low], axis=0), memory[i, h])
            got = got[0:1] + got[1:2]
            for b in range(hb):
                att[i * vb + h * hb + b : i * vb + h * hb + b + 1, :] = got[
                    :, b * LANES : (b + 1) * LANES
                ]
    pack1[...] = z_sum(zs1, zr1, nz)
    for i in range(2):
        at = i * slots_row
        value = pack1[at : at + vb, :] * inverse[i]
        gate = pack1[at + vb : at + 2 * vb, :] * inverse[i]
        attended = att[i * vb : (i + 1) * vb, :]
        for h in range(2):
            part = slice(h * hb, (h + 1) * hb)
            full = attended[part] + own[2 * i + h] * value[part]
            mean = jnp.sum(jnp.sum(full * full, axis=0, keepdims=True), axis=1, keepdims=True)
            norm = full * lax.rsqrt(mean * (1.0 / (hb * LANES)) + EPS) * hg[part, :]
            g = gate[part]
            headf[i * (headf.shape[0] // 2) + h * hb : i * (headf.shape[0] // 2) + (h + 1) * hb, :] = (
                g / (1.0 + jnp.exp(-g)) * norm
            )
    headb[kv, c] = headf[...].astype(BF16)

    def gather(buf, zs, xs, ps, rs, with_partner):
        mine = buf.at[kv, c]
        for k, zp in enumerate(far):
            send(mine, mine, zs.at[k], rs.at[kv, c], zp * NX + x, c)
        for k, xp in enumerate(sides):
            send(mine, mine, xs.at[z, k], rs.at[kv, c], z * NX + xp, c)
        if with_partner:
            send(mine, mine, ps.at[kv], rs.at[kv, c], kv, other)
        for zp in near:
            origin = zp * NX + x
            slot = buf.at[origin, c]
            remote(slot, slot, zs.at[0], rs.at[origin, c], origin, c).wait_recv()
            for k, xp in enumerate(sides):
                send(slot, slot, xs.at[zp, k], rs.at[origin, c], z * NX + xp, c)
            send(slot, slot, ps.at[origin], rs.at[origin, c], kv, other)
        for zp in [z] + near:
            for xp in sides[::-1]:
                origin = zp * NX + xp
                slot = buf.at[origin, c]
                remote(slot, slot, zs.at[0], rs.at[origin, c], z * NX + xp, c).wait_recv()
                send(slot, slot, ps.at[origin], rs.at[origin, c], kv, other)
        for zp in [z] + near:
            for xp in [x] + sides[::-1]:
                if zp is z and xp is x and not with_partner:
                    continue
                origin = zp * NX + xp
                slot = buf.at[origin, other]
                remote(slot, slot, zs.at[0], rs.at[origin, other], kv, other).wait_recv()

    gather(headb, hz, hx, hp, hr, True)

    n_kv = nz * NX
    hrows = headf.shape[0]
    headsf[...] = headb[...].astype(F32).reshape(headsf.shape)
    for cc in range(2):
        for b in range(vb):
            at = (cc * vb + b) * LANES
            for i in range(2):
                lhs[i * n_kv : (i + 1) * n_kv, at : at + LANES] = headsf[
                    pl.ds(cc * hrows + i * (hrows // 2) + b, n_kv, stride=2 * hrows), :
                ].astype(BF16)
    remote(wo.at[other], wo.at[other], psem.at[2], psem.at[3], kv, other).wait_recv()
    heads = lhs[:, : 2 * vb * LANES]
    projected = jnp.concatenate([dot(heads, wo[0]), dot(heads, wo[1])], axis=1)
    for i in range(2):
        old = tokf[pl.ds(i, n_kv, stride=2), :]
        whole[kv, i] = (old + projected[i * n_kv : (i + 1) * n_kv]).astype(BF16)

    gather(whole, az, ax, ap, ar, False)

    energy = jnp.zeros((2 * n_kv, LANES), F32)
    for k in range(n_kv):
        rows = jnp.concatenate([whole[k, 0], whole[k, 1]], axis=0).astype(F32)
        energy = energy + rows * rows
        cols = slice(k * LANES, (k + 1) * LANES)
        lhs[:, cols] = (rows * mlp_gain[:, cols].astype(F32)).astype(BF16)
    inv = lax.rsqrt(jnp.sum(energy, axis=1, keepdims=True) * (1.0 / width) + EPS)
    in_mlp[0].wait()
    gate = dot(lhs[:, :width], wmg[...]) * inv
    in_mlp[1].wait()
    up = dot(lhs[:, :width], wmu[...]) * inv
    hidden[...] = (gate / (1.0 + jnp.exp(-gate)) * up).astype(BF16)
    in_mlp[2].wait()
    hz_half = nz // 2
    for zh in range(2):
        for zi in range(hz_half):
            zp = zh * hz_half + zi
            part = dot(hidden[...], wmd[:, zp * NX * LANES : (zp + 1) * NX * LANES]).astype(BF16)
            for xp in range(NX):
                for i in range(2):
                    dpart[i, zh, xp, :, zi * LANES : (zi + 1) * LANES] = part[
                        i * n_kv : (i + 1) * n_kv, xp * LANES : (xp + 1) * LANES
                    ]
        send(dpart.at[other, zh], dpeer.at[zh], psem.at[4 + zh], psem.at[6 + zh], kv, other)
    for zh in range(2):
        remote(
            dpeer.at[zh], dpeer.at[zh], psem.at[4 + zh], psem.at[6 + zh], kv, other
        ).wait_recv()
        for xp in (xo, xr, xl, x):
            dx[xp, zh] = (dpart[c, zh, xp].astype(F32) + dpeer[zh, xp].astype(F32)).astype(BF16)
    x_first(dx, dra, drb, dsem, 0)
    x_second(dx, dra, drs, drb, dsem, 0)
    low_lanes = lax.broadcasted_iota(jnp.int32, (n_kv // 2, LANES), 1) < LANES // 2

    def squeeze(rows, right):
        top, bottom = rows[: n_kv // 2], rows[n_kv // 2 :]
        if right:
            top = pltpu.roll(top, LANES // 2, 1)
        else:
            bottom = pltpu.roll(bottom, LANES // 2, 1)
        return jnp.where(low_lanes, top, bottom)

    for hh, side in ((1, 0), (0, 1), (0, 0), (1, 1)):
        x_wait(drb, dsem, 0, side, hh)
    for zh in range(2):
        total = x_sum(dx, drb, zh)
        for zi in range(hz_half):
            rows = total[:, zi * LANES : (zi + 1) * LANES]
            for cc in range(2):
                dzs[zh * hz_half + zi, cc] = squeeze(rows, cc == 1).astype(BF16)
    for k, zp in enumerate(far):
        for q, cc in enumerate((other, c)):
            send(
                dzs.at[zp, cc],
                dzr.at[z, c],
                dzsem.at[0, k, q],
                dzsem.at[1, z, c],
                zp * NX + x,
                cc,
            )
    send(dzs.at[z, other], dzr.at[z, c], dzsem.at[0, nz - 1, 0], dzsem.at[1, z, c], kv, other)
    dzr[z, c] = dzs[z, c]
    for zp in [z] + near:
        for cc in (c, other):
            if zp is z and cc is c:
                continue
            slot = dzr.at[zp, cc]
            remote(
                slot, slot, dzsem.at[0, 0, 0], dzsem.at[1, zp, cc], zp * NX + x, cc
            ).wait_recv()
    for i in range(2):
        rows = whole[kv, i].astype(F32)
        total = jnp.where(c == 1, squeeze(rows, True), squeeze(rows, False))
        for zp in range(nz):
            total = total + dzr[zp, i].astype(F32)
        outf[pl.ds(i, n_kv // 2, stride=2), :] = total
        outf[pl.ds(i + n_kv, n_kv // 2, stride=2), :] = pltpu.roll(total, LANES // 2, 1)
    out[...] = outf[:, : LANES // 2].astype(BF16)
    for copy in sent:
        copy.wait_send()


def shards(
    tokens,
    lengths,
    state,
    cache_keys,
    cache_values,
    cache_rates,
    attn_gain,
    w_query,
    w_key,
    w_value,
    w_gate,
    w_decay,
    head_gain,
    w_out,
    mlp_gain,
    w_mlp_gate,
    w_mlp_up,
    w_mlp_down,
):
    n_kv = lax.axis_size("kv")
    nz = n_kv // NX
    heads, dk, dv = state.shape[1], state.shape[2], state.shape[3]
    width = mlp_gain.shape[0]
    qb, vb = heads * dk // LANES, heads * dv // LANES
    half0, half1 = (3 * qb + 2) // 2, vb
    slots = -(-2 * max(half0, half1) // 8) * 8
    rows2 = 2 * nz
    seqs = 2 * n_kv
    hrows = 2 * (-(-vb // 8) * 8)
    units = w_mlp_down.shape[0]
    cols5 = nz // 2 * LANES
    vmem, dma = pltpu.VMEM, pltpu.SemaphoreType.DMA
    bf, fl = BF16, F32
    scratch = [
        vmem((2, seqs, LANES // 2), bf),
        vmem((seqs, LANES), fl),
        vmem(w_query.shape, bf),
        vmem(w_key.shape, bf),
        vmem(w_decay.shape, bf),
        vmem(w_value.shape, bf),
        vmem(w_gate.shape, bf),
        vmem(state.shape, fl),
        vmem(cache_keys.shape, bf),
        vmem(cache_values.shape, bf),
        vmem(cache_rates.shape, fl),
        vmem((2,) + w_out.shape, bf),
        vmem(w_mlp_gate.shape, bf),
        vmem(w_mlp_up.shape, bf),
        vmem(w_mlp_down.shape, bf),
        vmem((NX, 2, rows2, half0 * LANES), bf),
        vmem((NX, 2, rows2, half1 * LANES), bf),
        vmem((2, rows2, half0 * LANES), bf),
        vmem((2, rows2, half1 * LANES), bf),
        vmem((2, rows2, half0 * LANES), bf),
        vmem((2, rows2, half1 * LANES), bf),
        vmem((2, 2, rows2, half0 * LANES), bf),
        vmem((2, 2, rows2, half1 * LANES), bf),
        vmem((rows2 * slots, LANES), fl),
        vmem((nz, 2 * slots, LANES), bf),
        vmem((nz, 2 * slots, LANES), bf),
        vmem((nz, 2 * slots, LANES), bf),
        vmem((nz, 2 * slots, LANES), bf),
        vmem(state.shape, bf),
        vmem((2 * slots, LANES), fl),
        vmem((2 * slots, LANES), fl),
        vmem((2 * qb, LANES), fl),
        vmem((2 * vb, LANES), fl),
        vmem((vb, LANES), fl),
        vmem((hrows, LANES), fl),
        vmem((n_kv, 2, hrows, LANES), bf),
        vmem((n_kv * 2 * hrows, LANES), fl),
        vmem((seqs, max(width, 2 * vb * LANES)), bf),
        vmem((n_kv, 2, n_kv, LANES), bf),
        vmem((seqs, units), bf),
        vmem((2, 2, NX, n_kv, cols5), bf),
        vmem((2, NX, n_kv, cols5), bf),
        vmem((NX, 2, n_kv, cols5), bf),
        vmem((2, n_kv, cols5), bf),
        vmem((2, n_kv, cols5), bf),
        vmem((2, 2, n_kv, cols5), bf),
        vmem((nz, 2, n_kv // 2, LANES), bf),
        vmem((nz, 2, n_kv // 2, LANES), bf),
        vmem((seqs, LANES), fl),
        dma((14,)),
        dma((8,)),
        dma((2, 12)),
        dma((2, 2 * nz)),
        dma((nz,)),
        dma((nz, NX)),
        dma((n_kv,)),
        dma((n_kv, 2)),
        dma((nz,)),
        dma((nz, NX)),
        dma((n_kv,)),
        dma((n_kv, 2)),
        dma((2, 6)),
        dma((2, nz, 2)),
    ]
    anywhere = pl.BlockSpec(memory_space=pl.ANY)
    in_vmem = pl.BlockSpec(memory_space=pltpu.VMEM)
    in_smem = pl.BlockSpec(memory_space=pltpu.SMEM)
    specs = [anywhere] * 18
    specs[1] = in_smem
    for k in (6, 12, 14):
        specs[k] = in_vmem
    return pl.pallas_call(
        functools.partial(kernel, (nz, qb, vb, dk, width)),
        out_shape=jax.ShapeDtypeStruct(tokens.shape, BF16),
        in_specs=specs,
        out_specs=in_vmem,
        scratch_shapes=scratch,
        compiler_params=pltpu.CompilerParams(collective_id=0, has_side_effects=True),
        name="layer",
    )(
        tokens,
        lengths,
        state,
        cache_keys,
        cache_values,
        cache_rates,
        attn_gain.reshape(1, -1),
        w_query,
        w_key,
        w_value,
        w_gate,
        w_decay,
        head_gain,
        w_out,
        mlp_gain.reshape(1, -1),
        w_mlp_gate,
        w_mlp_up,
        w_mlp_down,
    )


def solution(mesh):
    placed = (
        P("dp", ("kv", "tp")),
        P(("dp", "kv")),
        P(("dp", "kv"), "tp", None, None),
        P(("dp", "kv"), "tp", None, None),
        P(("dp", "kv"), "tp", None, None),
        P(("dp", "kv"), "tp", None, None),
        P("kv"),
        P("kv", "tp"),
        P("kv", "tp"),
        P("kv", "tp"),
        P("kv", "tp"),
        P("kv", "tp"),
        P("tp", None),
        P(None, ("kv", "tp")),
        P(),
        P(None, ("kv", "tp")),
        P(None, ("kv", "tp")),
        P(("kv", "tp"), None),
    )
    return jax.shard_map(
        shards, mesh=mesh, in_specs=placed, out_specs=P("dp", ("kv", "tp")), check_vma=False
    )
```

time: 140 us -> 75 us (0.54)
  Pallas kernels: 0 us -> 63.5 us
  waiting for transfers between devices: 52.2 us -> 0 us
  blocking collectives: 29.8 us -> 0 us
  starting transfers between devices: 22.1 us -> 0 us
  matrix products: 13.4 us -> 0 us
  local copies, waits for them, and re-layouts: 17.7 us -> 11.2 us
  other arithmetic: 4.14 us -> 0 us
    pallas_call x0 -> x1, Pallas kernels: none -> 63.5 us  [shards(): pl.pallas_call(functools.partial(kernel, (nz, qb, vb, dk, width)), out_sh...]
    all_to_all x3 -> x0, waiting for transfers between devices: 52.2 us -> none  [the longest x2 32.8 us: from_everyone(): return lax.all_to_all(copies, axis, split_axis=0, concat_axis=0, tiled=True)]
    all_to_all x2 -> x0, blocking collectives: 29.8 us -> none  [the longest x1 23.2 us: sum_at_owner(): parts = lax.all_to_all(cut_along(array, dim, size), axis, 0, 0, tiled=True)]
    all_to_all x3 -> x0, starting transfers between devices: 22.1 us -> none  [the longest x2 12.8 us: from_everyone(): return lax.all_to_all(copies, axis, split_axis=0, concat_axis=0, tiled=True)]
    dot_general x12 -> x0, matrix products: 13.4 us -> none  [the longest x1 4.71 us: front_part(): jnp.einsum('bhd,bhde->bhe', query * jnp.exp(log_decay - total[:, :, 0, :]...]
    convert_element_type x5 -> x0, local copies, waits for them, and re-layouts: 5 us -> none  [the longest x2 4.7 us: shards(): whole = gathered_copies(after, ('kv', 'tp'), 1).astype(jnp.float32)]
    unnamed x37 -> x6, local copies, waits for them, and re-layouts: 7.74 us -> 9.86 us
    broadcast_in_dim x3 -> x0, local copies, waits for them, and re-layouts: 2.05 us -> none  [from_everyone(): copies = jnp.broadcast_to(array, (lax.axis_size(axis), *array.shape))]
  transfers between devices with their start and end apart: 3 -> 0, of which waited for: 3 -> 0; matrix products, arithmetic and copies ran while one was open for 0% -> 0% of each run, Pallas kernels for 0% -> 0%
where the time goes in v1:
time: 75 us; the launch traced here: 74.7 us
  Pallas kernels  63.5 us (85%)
  local copies, waits for them, and re-layouts  11.2 us (15%)
    pallas_call x1, Pallas kernels, shards(): pl.pallas_call(functools.partial(kernel, (nz, qb, vb, dk, width)), out_sh...  63.5 us
    unnamed x6, local copies, waits for them, and re-layouts  9.86 us

profile of v1, /device:TPU:1, one launch (start us, length us, event | category | flops | bytes accessed | tf_op | source)
XLA Modules:
  0.0 74.7 jit_solution(6955153377391814748)
XLA Ops:
  0.0 1.3 %reshape.7.mlp_gain = bf16[1,4096]{1,0:T(2,128)(2,1)} reshape(bf16[4096]{0:T(1024)(128)(2,1)} %param.32) | data formatting | bytes 16384 | tf_op jit(solution)/shard_map/reshape | solution.py:645
  1.3 0.0 copy-start
  1.3 2.3 %copy.19.w_out = bf16[3072,64]{1,0:T(8,128)(2,1)} copy(bf16[3072,64]{0,1:T(8,128)(2,1)} %param.31) | data formatting | bytes 786432 | tf_op args[13]
  3.6 3.8 %copy.20.w_mlp_gate = bf16[4096,172]{1,0:T(8,128)(2,1)} copy(bf16[4096,172]{0,1:T(8,128)(2,1)} %param.33) | data formatting | bytes 2818048 | tf_op args[15]
  7.4 0.0 copy-done
  7.4 2.5 %copy.21.w_mlp_up = bf16[4096,172]{1,0:T(8,128)(2,1)} copy(bf16[4096,172]{0,1:T(8,128)(2,1)S(1)} %copy-done) | data formatting | bytes 2818048 | tf_op args[16]
  9.8 63.5 %layer.1 = bf16[64,64]{1,0:T(8,128)(2,1)} custom-call(bf16[64,64]{1,0:T(8,128)(2,1)} %tokens.1, s32[2]{0:T(128)} %lengths.1, f32[2,2,384,768]{3,2,1,0:T(8,128)} %state.1, bf16[2,2,64,384]{3,2,1,0:T(8,128)(2,1)} %cache_keys.1, bf16[2,2,64,768]{3,2,1,0:T(8,128)(2,1)} %cache_values.1, f32[2,2,64,384]{3,2,1,0:T(8,128)} %cache_rates.1, bf16[1,128]{1,0:T(2,128)(2,1)} %bitcast.1, ...), custom_call_target="tpu_custom_call" | custom-call | tf_op jit(solution)/shard_map/layer/pallas_call | solution.py:622
  73.3 1.3 %copy.23 = bf16[64,64]{1,0:T(8,128)(2,1)} copy(bf16[64,64]{1,0:T(8,128)(2,1)} %layer.1) | data formatting | bytes 16384
Async XLA Ops:
  1.3 6.1 %copy-start = (bf16[4096,172]{0,1:T(8,128)(2,1)S(1)}, bf16[4096,172]{0,1:T(8,128)(2,1)}, u32[]{:S(2)}) copy-start(bf16[4096,172]{0,1:T(8,128)(2,1)} %param.34) | copy-start | bytes 4227076

commit v2 on v1

--- a/solution.py
+++ b/solution.py
@@ -140,6 +140,15 @@
             device_id_type=MESH,
         )
 
+    scopes = []
+
+    def mark(name=None):
+        if scopes:
+            scopes.pop().__exit__(None, None, None)
+        if name:
+            scopes.append(jax.named_scope(name))
+            scopes[-1].__enter__()
+
     sent = []
 
     def send(*args):
@@ -147,6 +156,7 @@
         copy.start()
         sent.append(copy)
 
+    mark("load")
     in_tok = local(0, tokens, tok.at[c])
     in_w = [
         local(1 + i, src, dst)
@@ -165,6 +175,7 @@
         for i, (src, dst) in enumerate(((w_mlp_gate, wmg), (w_mlp_up, wmu), (w_mlp_down, wmd)))
     ]
 
+    mark("barrier")
     barrier = pltpu.get_barrier_semaphore()
 
     def greet(to_kv, to_tp):
@@ -186,6 +197,7 @@
             ].astype(F32)
     pl.semaphore_wait(barrier, 2 * len(far) + len(sides) + 1)
 
+    mark("tokens")
     in_tok.wait()
     send(tok.at[c], tok.at[c], psem.at[0], psem.at[1], kv, other)
     in_out.wait()
@@ -249,6 +261,7 @@
     def x_sum(src, back, half):
         return src[x, half].astype(F32) + back[0, half].astype(F32) + back[1, half].astype(F32)
 
+    mark("project_a")
     project(in_w[0], wq, x0, 0)
     project(in_w[1], wk, x0, qb)
     project(in_w[2], wd, x0, 2 * qb)
@@ -256,6 +269,7 @@
     for b in range(3 * qb + 1, 2 * (x0.shape[3] // LANES)):
         put(x0, b, jnp.zeros((squares.shape[0], LANES), F32))
     x_first(x0, ra0, rb0, xsem, 0)
+    mark("project_b")
     project(in_w[3], wv, x1, 0)
     project(in_w[4], wg, x1, vb)
     x_first(x1, ra1, rb1, xsem, 6)
@@ -283,6 +297,7 @@
             cols = slice(b * LANES, (b + 1) * LANES)
             memory[i, h, :, cols] = (st[i, h, :, cols] * shrink + inner[:, cols]).astype(BF16)
 
+    mark("x_second")
     for copy in in_cache:
         copy.wait()
     in_state.wait()
@@ -329,13 +344,18 @@
             total = total + landing[zp].astype(F32)
         return total
 
+    mark("z_send_a")
     z_send(x0, rb0, zs0, zr0, 0, 0)
+    mark("z_send_b")
     z_send(x1, rb1, zs1, zr1, 6, nz)
+    mark("fold")
     for i in range(2):
         for h in range(2):
             fold(i, h)
 
+    mark("z_wait_a")
     pack0[...] = z_sum(zs0, zr0, 0)
+    mark("heads_a")
     own = []
     inverse = []
     qh = qb // 2
@@ -364,9 +384,12 @@
                 att[i * vb + h * hb + b : i * vb + h * hb + b + 1, :] = got[
                     :, b * LANES : (b + 1) * LANES
                 ]
+    mark("z_wait_b")
     pack1[...] = z_sum(zs1, zr1, nz)
     for i in range(2):
         at = i * slots_row
+        if i == 0:
+            mark("heads_b")
         value = pack1[at : at + vb, :] * inverse[i]
         gate = pack1[at + vb : at + 2 * vb, :] * inverse[i]
         attended = att[i * vb : (i + 1) * vb, :]
@@ -410,8 +433,10 @@
                 slot = buf.at[origin, other]
                 remote(slot, slot, zs.at[0], rs.at[origin, other], kv, other).wait_recv()
 
+    mark("gather_heads")
     gather(headb, hz, hx, hp, hr, True)
 
+    mark("project_out")
     n_kv = nz * NX
     hrows = headf.shape[0]
     headsf[...] = headb[...].astype(F32).reshape(headsf.shape)
@@ -424,25 +449,28 @@
                 ].astype(BF16)
     remote(wo.at[other], wo.at[other], psem.at[2], psem.at[3], kv, other).wait_recv()
     heads = lhs[:, : 2 * vb * LANES]
-    projected = jnp.concatenate([dot(heads, wo[0]), dot(heads, wo[1])], axis=1)
+    projected = dot(heads, wo[...].reshape(LANES, 2 * vb * LANES), ((1,), (1,)))
     for i in range(2):
         old = tokf[pl.ds(i, n_kv, stride=2), :]
         whole[kv, i] = (old + projected[i * n_kv : (i + 1) * n_kv]).astype(BF16)
 
+    mark("gather_after")
     gather(whole, az, ax, ap, ar, False)
 
+    mark("mlp_in")
     energy = jnp.zeros((2 * n_kv, LANES), F32)
     for k in range(n_kv):
         rows = jnp.concatenate([whole[k, 0], whole[k, 1]], axis=0).astype(F32)
         energy = energy + rows * rows
         cols = slice(k * LANES, (k + 1) * LANES)
-        lhs[:, cols] = (rows * mlp_gain[:, cols].astype(F32)).astype(BF16)
+        lhs[:, cols] = (rows * mlp_gain[k : k + 1, :].astype(F32)).astype(BF16)
     inv = lax.rsqrt(jnp.sum(energy, axis=1, keepdims=True) * (1.0 / width) + EPS)
     in_mlp[0].wait()
-    gate = dot(lhs[:, :width], wmg[...]) * inv
+    gate = dot(lhs[:, :width], wmg[...], ((1,), (1,))) * inv
     in_mlp[1].wait()
-    up = dot(lhs[:, :width], wmu[...]) * inv
+    up = dot(lhs[:, :width], wmu[...], ((1,), (1,))) * inv
     hidden[...] = (gate / (1.0 + jnp.exp(-gate)) * up).astype(BF16)
+    mark("mlp_down")
     in_mlp[2].wait()
     hz_half = nz // 2
     for zh in range(2):
@@ -455,12 +483,14 @@
                         i * n_kv : (i + 1) * n_kv, xp * LANES : (xp + 1) * LANES
                     ]
         send(dpart.at[other, zh], dpeer.at[zh], psem.at[4 + zh], psem.at[6 + zh], kv, other)
+    mark("down_peer")
     for zh in range(2):
         remote(
             dpeer.at[zh], dpeer.at[zh], psem.at[4 + zh], psem.at[6 + zh], kv, other
         ).wait_recv()
         for xp in (xo, xr, xl, x):
             dx[xp, zh] = (dpart[c, zh, xp].astype(F32) + dpeer[zh, xp].astype(F32)).astype(BF16)
+    mark("down_x")
     x_first(dx, dra, drb, dsem, 0)
     x_second(dx, dra, drs, drb, dsem, 0)
     low_lanes = lax.broadcasted_iota(jnp.int32, (n_kv // 2, LANES), 1) < LANES // 2
@@ -473,8 +503,10 @@
             bottom = pltpu.roll(bottom, LANES // 2, 1)
         return jnp.where(low_lanes, top, bottom)
 
+    mark("down_x2")
     for hh, side in ((1, 0), (0, 1), (0, 0), (1, 1)):
         x_wait(drb, dsem, 0, side, hh)
+    mark("down_pack")
     for zh in range(2):
         total = x_sum(dx, drb, zh)
         for zi in range(hz_half):
@@ -493,6 +525,7 @@
             )
     send(dzs.at[z, other], dzr.at[z, c], dzsem.at[0, nz - 1, 0], dzsem.at[1, z, c], kv, other)
     dzr[z, c] = dzs[z, c]
+    mark("down_z")
     for zp in [z] + near:
         for cc in (c, other):
             if zp is z and cc is c:
@@ -501,6 +534,7 @@
             remote(
                 slot, slot, dzsem.at[0, 0, 0], dzsem.at[1, zp, cc], zp * NX + x, cc
             ).wait_recv()
+    mark("finish")
     for i in range(2):
         rows = whole[kv, i].astype(F32)
         total = jnp.where(c == 1, squeeze(rows, True), squeeze(rows, False))
@@ -509,8 +543,10 @@
         outf[pl.ds(i, n_kv // 2, stride=2), :] = total
         outf[pl.ds(i + n_kv, n_kv // 2, stride=2), :] = pltpu.roll(total, LANES // 2, 1)
     out[...] = outf[:, : LANES // 2].astype(BF16)
+    mark("drain")
     for copy in sent:
         copy.wait_send()
+    mark()
 
 
 def shards(
@@ -559,9 +595,9 @@
         vmem(cache_keys.shape, bf),
         vmem(cache_values.shape, bf),
         vmem(cache_rates.shape, fl),
-        vmem((2,) + w_out.shape, bf),
-        vmem(w_mlp_gate.shape, bf),
-        vmem(w_mlp_up.shape, bf),
+        vmem((2,) + w_out.shape[::-1], bf),
+        vmem(w_mlp_gate.shape[::-1], bf),
+        vmem(w_mlp_up.shape[::-1], bf),
         vmem(w_mlp_down.shape, bf),
         vmem((NX, 2, rows2, half0 * LANES), bf),
         vmem((NX, 2, rows2, half1 * LANES), bf),
@@ -641,10 +677,10 @@
         w_gate,
         w_decay,
         head_gain,
-        w_out,
-        mlp_gain.reshape(1, -1),
-        w_mlp_gate,
-        w_mlp_up,
+        w_out.T,
+        mlp_gain.reshape(-1, LANES),
+        w_mlp_gate.T,
+        w_mlp_up.T,
         w_mlp_down,
     )
 

time: 75 us -> 65.4 us (0.87)
  local copies, waits for them, and re-layouts: 11.2 us -> 1.32 us
    unnamed x6 -> x1, local copies, waits for them, and re-layouts: 9.86 us -> 1.32 us
    reshape x1 -> x0, local copies, waits for them, and re-layouts: 1.31 us -> none  [shards(): mlp_gain.reshape(1, -1)]
where the time goes in v2:
time: 65.4 us; the launch traced here: 65.2 us
  Pallas kernels  63.9 us (98%)
  local copies, waits for them, and re-layouts  1.32 us (2%)
    pallas_call x1, Pallas kernels, shards(): pl.pallas_call(functools.partial(kernel, (nz, qb, vb, dk, width)), out_sh...  63.9 us
    unnamed x1, local copies, waits for them, and re-layouts  1.32 us

profile of v2, /device:TPU:1, one launch (start us, length us, event | category | flops | bytes accessed | tf_op | source)
XLA Modules:
  0.0 65.2 jit_solution(10894823771368680356)
XLA Ops:
  0.0 63.9 %layer.1 = bf16[64,64]{1,0:T(8,128)(2,1)} custom-call(bf16[64,64]{1,0:T(8,128)(2,1)} %tokens.1, s32[2]{0:T(128)} %lengths.1, f32[2,2,384,768]{3,2,1,0:T(8,128)} %state.1, bf16[2,2,64,384]{3,2,1,0:T(8,128)(2,1)} %cache_keys.1, bf16[2,2,64,768]{3,2,1,0:T(8,128)(2,1)} %cache_values.1, f32[2,2,64,384]{3,2,1,0:T(8,128)} %cache_rates.1, bf16[1,128]{1,0:T(2,128)(2,1)} %bitcast.9, ...), custom_call_target="tpu_custom_call" | custom-call | tf_op jit(solution)/shard_map/layer/pallas_call | solution.py:658
  63.9 1.3 %copy.20 = bf16[64,64]{1,0:T(8,128)(2,1)} copy(bf16[64,64]{1,0:T(8,128)(2,1)} %layer.1) | data formatting | bytes 16384

commit v3 on v2

--- a/solution.py
+++ b/solution.py
@@ -95,19 +95,17 @@
     dzs,
     dzr,
     outf,
+    again,
+    hgain,
+    mgain,
+    mgainf,
+    lens,
     lsem,
     psem,
     xsem,
     zsem,
-    hz,
-    hx,
-    hp,
-    hr,
-    az,
-    ax,
-    ap,
-    ar,
-    dsem,
+    hsem,
+    asem,
     dzsem,
 ):
     nz, qb, vb, dk, width = sizes
@@ -149,15 +147,17 @@
             scopes.append(jax.named_scope(name))
             scopes[-1].__enter__()
 
-    sent = []
-
     def send(*args):
-        copy = remote(*args)
-        copy.start()
-        sent.append(copy)
+        remote(*args).start()
 
     mark("load")
     in_tok = local(0, tokens, tok.at[c])
+    in_small = [
+        local(14 + i, src, dst)
+        for i, (src, dst) in enumerate(
+            ((attn_gain, again), (head_gain, hgain), (mlp_gain, mgain), (lengths, lens))
+        )
+    ]
     in_w = [
         local(1 + i, src, dst)
         for i, (src, dst) in enumerate(
@@ -190,9 +190,12 @@
         greet(z * NX + xp, c)
     greet(kv, other)
     zf[...] = jnp.zeros_like(zf)
+    for copy in in_small:
+        copy.wait()
+    mgainf[...] = mgain[...].astype(F32)
     for h in range(2):
         for b in range(vb // 2):
-            hg[h * (vb // 2) + b : h * (vb // 2) + b + 1, :] = head_gain[
+            hg[h * (vb // 2) + b : h * (vb // 2) + b + 1, :] = hgain[
                 h : h + 1, b * LANES : (b + 1) * LANES
             ].astype(F32)
     pl.semaphore_wait(barrier, 2 * len(far) + len(sides) + 1)
@@ -213,13 +216,13 @@
         axis=0,
     )
     squares = jnp.sum(block * block, axis=1, keepdims=True)
-    scaled = (block * attn_gain[...].astype(F32)).astype(BF16)
+    scaled = (block * again[...].astype(F32)).astype(BF16)
 
     def put(target, b, values):
-        half = target.shape[3] // LANES
+        half = target.shape[2] // LANES
         at = (b % half) * LANES
         for xp in range(NX):
-            target[xp, b // half, :, at : at + LANES] = values[
+            target[2 * xp + b // half, :, at : at + LANES] = values[
                 xp * rows2 : (xp + 1) * rows2
             ].astype(BF16)
 
@@ -229,50 +232,47 @@
         for b in range(weight.shape[1] // LANES):
             put(target, start + b, part[:, b * LANES : (b + 1) * LANES])
 
-    def x_first(src, first, back, sems, base):
-        send(src.at[xo, 0], first.at[0], sems.at[0, base], sems.at[1, base], z * NX + xr, c)
-        send(src.at[xo, 1], first.at[1], sems.at[0, base + 1], sems.at[1, base + 1], z * NX + xl, c)
-        send(src.at[xr, 1], back.at[0, 1], sems.at[0, base + 2], sems.at[1, base + 2], z * NX + xr, c)
-        send(src.at[xl, 0], back.at[1, 0], sems.at[0, base + 3], sems.at[1, base + 3], z * NX + xl, c)
-
-    def x_second(src, first, relay, back, sems, base):
-        remote(
-            first.at[0], first.at[0], sems.at[0, base], sems.at[1, base], z * NX + xl, c
-        ).wait_recv()
-        relay[0] = (src[xr, 0].astype(F32) + first[0].astype(F32)).astype(BF16)
-        send(relay.at[0], back.at[0, 0], sems.at[0, base + 4], sems.at[1, base + 4], z * NX + xr, c)
-        remote(
-            first.at[1], first.at[1], sems.at[0, base + 1], sems.at[1, base + 1], z * NX + xr, c
-        ).wait_recv()
-        relay[1] = (src[xl, 1].astype(F32) + first[1].astype(F32)).astype(BF16)
-        send(relay.at[1], back.at[1, 1], sems.at[0, base + 5], sems.at[1, base + 5], z * NX + xl, c)
-
-    def x_wait(back, sems, base, side, half):
-        slot = {(0, 1): 2, (1, 0): 3, (0, 0): 4, (1, 1): 5}[(side, half)]
-        remote(
-            back.at[side, half],
-            back.at[side, half],
-            sems.at[0, base + slot],
-            sems.at[1, base + slot],
-            z * NX + (xr if side else xl),
-            c,
-        ).wait_recv()
+    left, right = z * NX + xl, z * NX + xr
+
+    def x_first(src, first, back, stage):
+        out_sem, in_left, in_right, in_back = [xsem.at[stage, k] for k in range(4)]
+        send(src.at[2 * xo], first.at[0], out_sem, in_left, right, c)
+        send(src.at[2 * xo + 1], first.at[1], out_sem, in_right, left, c)
+        send(src.at[2 * xr + 1], back.at[1], out_sem, in_back, right, c)
+        send(src.at[2 * xl], back.at[2], out_sem, in_back, left, c)
+
+    def x_second(src, first, relay, back, stage):
+        out_sem, in_left, in_right, in_back = [xsem.at[stage, k] for k in range(4)]
+        remote(first.at[0], first.at[0], out_sem, in_left, left, c).wait_recv()
+        relay[0] = (src[2 * xr].astype(F32) + first[0].astype(F32)).astype(BF16)
+        send(relay.at[0], back.at[0], out_sem, in_back, right, c)
+        remote(first.at[1], first.at[1], out_sem, in_right, right, c).wait_recv()
+        relay[1] = (src[2 * xl + 1].astype(F32) + first[1].astype(F32)).astype(BF16)
+        send(relay.at[1], back.at[3], out_sem, in_back, left, c)
+
+    def x_wait(back, stage):
+        remote(back, back, xsem.at[stage, 0], xsem.at[stage, 3], left, c).wait_recv()
+
+    def x_drain(src, stage):
+        part = src.at[pl.ds(0, 6)]
+        remote(part, part, xsem.at[stage, 0], xsem.at[stage, 3], left, c).wait_send()
 
     def x_sum(src, back, half):
-        return src[x, half].astype(F32) + back[0, half].astype(F32) + back[1, half].astype(F32)
-
-    mark("project_a")
+        return (
+            src[2 * x + half].astype(F32) + back[half].astype(F32) + back[2 + half].astype(F32)
+        )
+
     project(in_w[0], wq, x0, 0)
     project(in_w[1], wk, x0, qb)
     project(in_w[2], wd, x0, 2 * qb)
     put(x0, 3 * qb, jnp.broadcast_to(squares, (squares.shape[0], LANES)))
-    for b in range(3 * qb + 1, 2 * (x0.shape[3] // LANES)):
+    for b in range(3 * qb + 1, 2 * (x0.shape[2] // LANES)):
         put(x0, b, jnp.zeros((squares.shape[0], LANES), F32))
-    x_first(x0, ra0, rb0, xsem, 0)
+    x_first(x0, ra0, rb0, 0)
     mark("project_b")
     project(in_w[3], wv, x1, 0)
     project(in_w[4], wg, x1, vb)
-    x_first(x1, ra1, rb1, xsem, 6)
+    x_first(x1, ra1, rb1, 1)
 
     span = ck.shape[2]
     hb = vb // 2
@@ -284,7 +284,7 @@
     slots = lax.broadcasted_iota(jnp.int32, (span, 1), 0)
 
     def fold(i, h):
-        live = (slots < lengths[i]).astype(F32)
+        live = (slots < lens[i]).astype(F32)
         rates = cr[i, h] * live
         high, low = high_low(rates)
         rest = dot(later, high) + dot(later, low)
@@ -301,15 +301,14 @@
     for copy in in_cache:
         copy.wait()
     in_state.wait()
-    x_second(x0, ra0, rs0, rb0, xsem, 0)
-    x_second(x1, ra1, rs1, rb1, xsem, 6)
+    x_second(x0, ra0, rs0, rb0, 0)
+    x_second(x1, ra1, rs1, rb1, 1)
 
     slots_row = zf.shape[0] // rows2
 
-    def z_send(src, back, packed, landing, base, sem_base):
-        half = src.shape[3] // LANES
-        for hh, side in ((1, 0), (0, 1), (0, 0), (1, 1)):
-            x_wait(back, xsem, base, side, hh)
+    def z_send(src, back, packed, landing, stage):
+        half = src.shape[2] // LANES
+        x_wait(back, stage)
         for hh in (0, 1):
             total = x_sum(src, back, hh)
             for b in range(half):
@@ -319,35 +318,23 @@
                     ]
         for zp in range(nz):
             packed[zp] = zf[zp * 2 * slots_row : (zp + 1) * 2 * slots_row, :].astype(BF16)
-        for k, zp in enumerate(far):
+        for zp in far:
             send(
-                packed.at[zp],
-                landing.at[z],
-                zsem.at[0, sem_base + k],
-                zsem.at[1, sem_base + z],
-                zp * NX + x,
-                c,
+                packed.at[zp], landing.at[z], zsem.at[stage, 0], zsem.at[stage, 1], zp * NX + x, c
             )
 
-    def z_sum(packed, landing, sem_base):
-        for zp in near:
-            remote(
-                landing.at[zp],
-                landing.at[zp],
-                zsem.at[0, sem_base],
-                zsem.at[1, sem_base + zp],
-                zp * NX + x,
-                c,
-            ).wait_recv()
+    def z_sum(packed, landing, stage):
+        part = landing.at[pl.ds(0, nz - 1)]
+        remote(part, part, zsem.at[stage, 0], zsem.at[stage, 1], left, c).wait_recv()
         total = packed[z].astype(F32)
         for zp in near:
             total = total + landing[zp].astype(F32)
         return total
 
     mark("z_send_a")
-    z_send(x0, rb0, zs0, zr0, 0, 0)
+    z_send(x0, rb0, zs0, zr0, 0)
     mark("z_send_b")
-    z_send(x1, rb1, zs1, zr1, 6, nz)
+    z_send(x1, rb1, zs1, zr1, 1)
     mark("fold")
     for i in range(2):
         for h in range(2):
@@ -385,7 +372,7 @@
                     :, b * LANES : (b + 1) * LANES
                 ]
     mark("z_wait_b")
-    pack1[...] = z_sum(zs1, zr1, nz)
+    pack1[...] = z_sum(zs1, zr1, 1)
     for i in range(2):
         at = i * slots_row
         if i == 0:
@@ -402,44 +389,57 @@
             headf[i * (headf.shape[0] // 2) + h * hb : i * (headf.shape[0] // 2) + (h + 1) * hb, :] = (
                 g / (1.0 + jnp.exp(-g)) * norm
             )
-    headb[kv, c] = headf[...].astype(BF16)
-
-    def gather(buf, zs, xs, ps, rs, with_partner):
-        mine = buf.at[kv, c]
-        for k, zp in enumerate(far):
-            send(mine, mine, zs.at[k], rs.at[kv, c], zp * NX + x, c)
-        for k, xp in enumerate(sides):
-            send(mine, mine, xs.at[z, k], rs.at[kv, c], z * NX + xp, c)
+    headb[2 * kv + c] = headf[...].astype(BF16)
+
+    def gather(buf, sems, with_partner, consume):
+        out_sem = sems.at[0]
+        mine = buf.at[2 * kv + c]
+        for zp in far:
+            send(mine, mine, out_sem, sems.at[1 + z], zp * NX + x, c)
+        for xp in sides:
+            send(mine, mine, out_sem, sems.at[1 + nz + z], z * NX + xp, c)
         if with_partner:
-            send(mine, mine, ps.at[kv], rs.at[kv, c], kv, other)
+            send(mine, mine, out_sem, sems.at[1 + 2 * nz + z], kv, other)
         for zp in near:
             origin = zp * NX + x
-            slot = buf.at[origin, c]
-            remote(slot, slot, zs.at[0], rs.at[origin, c], origin, c).wait_recv()
-            for k, xp in enumerate(sides):
-                send(slot, slot, xs.at[zp, k], rs.at[origin, c], z * NX + xp, c)
-            send(slot, slot, ps.at[origin], rs.at[origin, c], kv, other)
-        for zp in [z] + near:
+            slot = buf.at[2 * origin + c]
+            remote(slot, slot, out_sem, sems.at[1 + zp], origin, c).wait_recv()
+            for xp in sides:
+                send(slot, slot, out_sem, sems.at[1 + nz + zp], z * NX + xp, c)
+            send(slot, slot, out_sem, sems.at[1 + 2 * nz + zp], kv, other)
+        order = [z] + near
+
+        def finish(zp):
+            part = buf.at[pl.ds(0, NX - (zp is z and not with_partner))]
+            remote(part, part, out_sem, sems.at[1 + 2 * nz + zp], kv, other).wait_recv()
+            consume(zp)
+
+        for n, zp in enumerate(order):
+            part = buf.at[pl.ds(0, NX - 1)]
+            remote(part, part, out_sem, sems.at[1 + nz + zp], left, c).wait_recv()
             for xp in sides[::-1]:
-                origin = zp * NX + xp
-                slot = buf.at[origin, c]
-                remote(slot, slot, zs.at[0], rs.at[origin, c], z * NX + xp, c).wait_recv()
-                send(slot, slot, ps.at[origin], rs.at[origin, c], kv, other)
-        for zp in [z] + near:
-            for xp in [x] + sides[::-1]:
-                if zp is z and xp is x and not with_partner:
-                    continue
-                origin = zp * NX + xp
-                slot = buf.at[origin, other]
-                remote(slot, slot, zs.at[0], rs.at[origin, other], kv, other).wait_recv()
-
-    mark("gather_heads")
-    gather(headb, hz, hx, hp, hr, True)
-
-    mark("project_out")
+                slot = buf.at[2 * (zp * NX + xp) + c]
+                send(slot, slot, out_sem, sems.at[1 + 2 * nz + zp], kv, other)
+            if n:
+                finish(order[n - 1])
+        finish(order[-1])
+
+    def gather_drain(buf, sems, with_partner):
+        part = buf.at[pl.ds(0, 2 * nz * NX - 1 - (not with_partner))]
+        remote(part, part, sems.at[0], sems.at[1], left, c).wait_send()
+
     n_kv = nz * NX
     hrows = headf.shape[0]
-    headsf[...] = headb[...].astype(F32).reshape(headsf.shape)
+
+    def widen(zp):
+        for k in range(2 * NX):
+            slot = 2 * NX * zp + k
+            headsf[pl.ds(pl.multiple_of(slot * hrows, 8), hrows), :] = headb[slot].astype(F32)
+
+    mark("gather_heads")
+    gather(headb, hsem, True, widen)
+
+    mark("project_out")
     for cc in range(2):
         for b in range(vb):
             at = (cc * vb + b) * LANES
@@ -448,27 +448,38 @@
                     pl.ds(cc * hrows + i * (hrows // 2) + b, n_kv, stride=2 * hrows), :
                 ].astype(BF16)
     remote(wo.at[other], wo.at[other], psem.at[2], psem.at[3], kv, other).wait_recv()
-    heads = lhs[:, : 2 * vb * LANES]
-    projected = dot(heads, wo[...].reshape(LANES, 2 * vb * LANES), ((1,), (1,)))
+    projected = dot(lhs[...], wo[...].reshape(LANES, 2 * vb * LANES), ((1,), (1,)))
     for i in range(2):
         old = tokf[pl.ds(i, n_kv, stride=2), :]
-        whole[kv, i] = (old + projected[i * n_kv : (i + 1) * n_kv]).astype(BF16)
+        whole[2 * kv + i] = (old + projected[i * n_kv : (i + 1) * n_kv]).astype(BF16)
 
     mark("gather_after")
-    gather(whole, az, ax, ap, ar, False)
+    in_mlp[0].wait()
+    in_mlp[1].wait()
+    sums = [
+        jnp.zeros((2 * n_kv, LANES), F32),
+        jnp.zeros(hidden.shape, F32),
+        jnp.zeros(hidden.shape, F32),
+    ]
+
+    def multiply(zp):
+        parts = []
+        for xp in range(NX):
+            k = zp * NX + xp
+            rows = jnp.concatenate([whole[2 * k], whole[2 * k + 1]], axis=0).astype(F32)
+            sums[0] = sums[0] + rows * rows
+            parts.append((rows * mgainf[pl.ds(k, 1), :]).astype(BF16))
+        rows = jnp.concatenate(parts, axis=1)
+        cols = pl.ds(pl.multiple_of(zp * NX * LANES, LANES), NX * LANES)
+        sums[1] = sums[1] + dot(rows, wmg[:, cols], ((1,), (1,)))
+        sums[2] = sums[2] + dot(rows, wmu[:, cols], ((1,), (1,)))
+
+    gather(whole, asem, False, multiply)
 
     mark("mlp_in")
-    energy = jnp.zeros((2 * n_kv, LANES), F32)
-    for k in range(n_kv):
-        rows = jnp.concatenate([whole[k, 0], whole[k, 1]], axis=0).astype(F32)
-        energy = energy + rows * rows
-        cols = slice(k * LANES, (k + 1) * LANES)
-        lhs[:, cols] = (rows * mlp_gain[k : k + 1, :].astype(F32)).astype(BF16)
-    inv = lax.rsqrt(jnp.sum(energy, axis=1, keepdims=True) * (1.0 / width) + EPS)
-    in_mlp[0].wait()
-    gate = dot(lhs[:, :width], wmg[...], ((1,), (1,))) * inv
-    in_mlp[1].wait()
-    up = dot(lhs[:, :width], wmu[...], ((1,), (1,))) * inv
+    inv = lax.rsqrt(jnp.sum(sums[0], axis=1, keepdims=True) * (1.0 / width) + EPS)
+    gate = sums[1] * inv
+    up = sums[2] * inv
     hidden[...] = (gate / (1.0 + jnp.exp(-gate)) * up).astype(BF16)
     mark("mlp_down")
     in_mlp[2].wait()
@@ -482,17 +493,17 @@
                     dpart[i, zh, xp, :, zi * LANES : (zi + 1) * LANES] = part[
                         i * n_kv : (i + 1) * n_kv, xp * LANES : (xp + 1) * LANES
                     ]
-        send(dpart.at[other, zh], dpeer.at[zh], psem.at[4 + zh], psem.at[6 + zh], kv, other)
+        send(dpart.at[other, zh], dpeer.at[zh], psem.at[4], psem.at[5 + zh], kv, other)
     mark("down_peer")
     for zh in range(2):
         remote(
-            dpeer.at[zh], dpeer.at[zh], psem.at[4 + zh], psem.at[6 + zh], kv, other
+            dpeer.at[zh], dpeer.at[zh], psem.at[4], psem.at[5 + zh], kv, other
         ).wait_recv()
         for xp in (xo, xr, xl, x):
-            dx[xp, zh] = (dpart[c, zh, xp].astype(F32) + dpeer[zh, xp].astype(F32)).astype(BF16)
+            dx[2 * xp + zh] = (dpart[c, zh, xp].astype(F32) + dpeer[zh, xp].astype(F32)).astype(BF16)
     mark("down_x")
-    x_first(dx, dra, drb, dsem, 0)
-    x_second(dx, dra, drs, drb, dsem, 0)
+    x_first(dx, dra, drb, 2)
+    x_second(dx, dra, drs, drb, 2)
     low_lanes = lax.broadcasted_iota(jnp.int32, (n_kv // 2, LANES), 1) < LANES // 2
 
     def squeeze(rows, right):
@@ -504,48 +515,52 @@
         return jnp.where(low_lanes, top, bottom)
 
     mark("down_x2")
-    for hh, side in ((1, 0), (0, 1), (0, 0), (1, 1)):
-        x_wait(drb, dsem, 0, side, hh)
+    x_wait(drb, 2)
     mark("down_pack")
     for zh in range(2):
         total = x_sum(dx, drb, zh)
         for zi in range(hz_half):
             rows = total[:, zi * LANES : (zi + 1) * LANES]
             for cc in range(2):
-                dzs[zh * hz_half + zi, cc] = squeeze(rows, cc == 1).astype(BF16)
-    for k, zp in enumerate(far):
-        for q, cc in enumerate((other, c)):
+                dzs[2 * (zh * hz_half + zi) + cc] = squeeze(rows, cc == 1).astype(BF16)
+    for zp in far:
+        for cc in (other, c):
             send(
-                dzs.at[zp, cc],
-                dzr.at[z, c],
-                dzsem.at[0, k, q],
-                dzsem.at[1, z, c],
+                dzs.at[2 * zp + cc],
+                dzr.at[2 * z + c],
+                dzsem.at[0],
+                dzsem.at[1],
                 zp * NX + x,
                 cc,
             )
-    send(dzs.at[z, other], dzr.at[z, c], dzsem.at[0, nz - 1, 0], dzsem.at[1, z, c], kv, other)
-    dzr[z, c] = dzs[z, c]
+    send(dzs.at[2 * z + other], dzr.at[2 * z + c], dzsem.at[0], dzsem.at[1], kv, other)
+    dzr[2 * z + c] = dzs[2 * z + c]
     mark("down_z")
-    for zp in [z] + near:
-        for cc in (c, other):
-            if zp is z and cc is c:
-                continue
-            slot = dzr.at[zp, cc]
-            remote(
-                slot, slot, dzsem.at[0, 0, 0], dzsem.at[1, zp, cc], zp * NX + x, cc
-            ).wait_recv()
+    part = dzr.at[pl.ds(0, 2 * nz - 1)]
+    remote(part, part, dzsem.at[0], dzsem.at[1], kv, other).wait_recv()
     mark("finish")
     for i in range(2):
-        rows = whole[kv, i].astype(F32)
+        rows = whole[2 * kv + i].astype(F32)
         total = jnp.where(c == 1, squeeze(rows, True), squeeze(rows, False))
         for zp in range(nz):
-            total = total + dzr[zp, i].astype(F32)
+            total = total + dzr[2 * zp + i].astype(F32)
         outf[pl.ds(i, n_kv // 2, stride=2), :] = total
         outf[pl.ds(i + n_kv, n_kv // 2, stride=2), :] = pltpu.roll(total, LANES // 2, 1)
     out[...] = outf[:, : LANES // 2].astype(BF16)
     mark("drain")
-    for copy in sent:
-        copy.wait_send()
+    remote(tok.at[c], tok.at[c], psem.at[0], psem.at[1], kv, other).wait_send()
+    remote(wo.at[c], wo.at[c], psem.at[2], psem.at[3], kv, other).wait_send()
+    x_drain(x0, 0)
+    x_drain(x1, 1)
+    for stage, landing in enumerate((zr0, zr1)):
+        part = landing.at[pl.ds(0, nz - 1)]
+        remote(part, part, zsem.at[stage, 0], zsem.at[stage, 1], left, c).wait_send()
+    gather_drain(headb, hsem, True)
+    gather_drain(whole, asem, False)
+    remote(dpeer, dpeer, psem.at[4], psem.at[5], kv, other).wait_send()
+    x_drain(dx, 2)
+    part = dzr.at[pl.ds(0, 2 * nz - 1)]
+    remote(part, part, dzsem.at[0], dzsem.at[1], kv, other).wait_send()
     mark()
 
 
@@ -578,7 +593,7 @@
     slots = -(-2 * max(half0, half1) // 8) * 8
     rows2 = 2 * nz
     seqs = 2 * n_kv
-    hrows = 2 * (-(-vb // 8) * 8)
+    hrows = 2 * vb
     units = w_mlp_down.shape[0]
     cols5 = nz // 2 * LANES
     vmem, dma = pltpu.VMEM, pltpu.SemaphoreType.DMA
@@ -599,14 +614,14 @@
         vmem(w_mlp_gate.shape[::-1], bf),
         vmem(w_mlp_up.shape[::-1], bf),
         vmem(w_mlp_down.shape, bf),
-        vmem((NX, 2, rows2, half0 * LANES), bf),
-        vmem((NX, 2, rows2, half1 * LANES), bf),
+        vmem((NX * 2, rows2, half0 * LANES), bf),
+        vmem((NX * 2, rows2, half1 * LANES), bf),
         vmem((2, rows2, half0 * LANES), bf),
         vmem((2, rows2, half1 * LANES), bf),
         vmem((2, rows2, half0 * LANES), bf),
         vmem((2, rows2, half1 * LANES), bf),
-        vmem((2, 2, rows2, half0 * LANES), bf),
-        vmem((2, 2, rows2, half1 * LANES), bf),
+        vmem((4, rows2, half0 * LANES), bf),
+        vmem((4, rows2, half1 * LANES), bf),
         vmem((rows2 * slots, LANES), fl),
         vmem((nz, 2 * slots, LANES), bf),
         vmem((nz, 2 * slots, LANES), bf),
@@ -619,42 +634,36 @@
         vmem((2 * vb, LANES), fl),
         vmem((vb, LANES), fl),
         vmem((hrows, LANES), fl),
-        vmem((n_kv, 2, hrows, LANES), bf),
+        vmem((2 * n_kv, hrows, LANES), bf),
         vmem((n_kv * 2 * hrows, LANES), fl),
-        vmem((seqs, max(width, 2 * vb * LANES)), bf),
-        vmem((n_kv, 2, n_kv, LANES), bf),
+        vmem((seqs, 2 * vb * LANES), bf),
+        vmem((2 * n_kv, n_kv, LANES), bf),
         vmem((seqs, units), bf),
         vmem((2, 2, NX, n_kv, cols5), bf),
         vmem((2, NX, n_kv, cols5), bf),
-        vmem((NX, 2, n_kv, cols5), bf),
+        vmem((NX * 2, n_kv, cols5), bf),
         vmem((2, n_kv, cols5), bf),
         vmem((2, n_kv, cols5), bf),
-        vmem((2, 2, n_kv, cols5), bf),
-        vmem((nz, 2, n_kv // 2, LANES), bf),
-        vmem((nz, 2, n_kv // 2, LANES), bf),
+        vmem((4, n_kv, cols5), bf),
+        vmem((2 * nz, n_kv // 2, LANES), bf),
+        vmem((2 * nz, n_kv // 2, LANES), bf),
         vmem((seqs, LANES), fl),
-        dma((14,)),
-        dma((8,)),
-        dma((2, 12)),
-        dma((2, 2 * nz)),
-        dma((nz,)),
-        dma((nz, NX)),
-        dma((n_kv,)),
-        dma((n_kv, 2)),
-        dma((nz,)),
-        dma((nz, NX)),
-        dma((n_kv,)),
-        dma((n_kv, 2)),
-        dma((2, 6)),
-        dma((2, nz, 2)),
+        vmem((1, LANES), bf),
+        vmem((heads, dv), bf),
+        vmem((n_kv, LANES), bf),
+        vmem((n_kv, LANES), fl),
+        pltpu.SMEM((2,), jnp.int32),
+        dma((18,)),
+        dma((7,)),
+        dma((3, 4)),
+        dma((2, 2)),
+        dma((1 + 3 * nz,)),
+        dma((1 + 3 * nz,)),
+        dma((2,)),
     ]
     anywhere = pl.BlockSpec(memory_space=pl.ANY)
     in_vmem = pl.BlockSpec(memory_space=pltpu.VMEM)
-    in_smem = pl.BlockSpec(memory_space=pltpu.SMEM)
     specs = [anywhere] * 18
-    specs[1] = in_smem
-    for k in (6, 12, 14):
-        specs[k] = in_vmem
     return pl.pallas_call(
         functools.partial(kernel, (nz, qb, vb, dk, width)),
         out_shape=jax.ShapeDtypeStruct(tokens.shape, BF16),

time: 65.4 us -> 63 us (0.963)
  Pallas kernels: 63.9 us -> 61.5 us
    pallas_call x1, Pallas kernels: 63.9 us -> 61.5 us  [shards(): pl.pallas_call(functools.partial(kernel, (nz, qb, vb, dk, width)), out_sh...]
where the time goes in v3:
time: 63 us; the launch traced here: 62.9 us
  Pallas kernels  61.5 us (98%)
  local copies, waits for them, and re-layouts  1.32 us (2%)
    pallas_call x1, Pallas kernels, shards(): pl.pallas_call(functools.partial(kernel, (nz, qb, vb, dk, width)), out_sh...  61.5 us
    unnamed x1, local copies, waits for them, and re-layouts  1.32 us

profile of v3, /device:TPU:1, one launch (start us, length us, event | category | flops | bytes accessed | tf_op | source)
XLA Modules:
  0.0 62.9 jit_solution(215044944520072466)
XLA Ops:
  0.0 61.5 %layer.1 = bf16[64,64]{1,0:T(8,128)(2,1)} custom-call(bf16[64,64]{1,0:T(8,128)(2,1)} %tokens.1, s32[2]{0:T(128)} %lengths.1, f32[2,2,384,768]{3,2,1,0:T(8,128)} %state.1, bf16[2,2,64,384]{3,2,1,0:T(8,128)(2,1)} %cache_keys.1, bf16[2,2,64,768]{3,2,1,0:T(8,128)(2,1)} %cache_values.1, f32[2,2,64,384]{3,2,1,0:T(8,128)} %cache_rates.1, bf16[1,128]{1,0:T(2,128)(2,1)} %bitcast.9, ...), custom_call_target="tpu_custom_call" | custom-call | tf_op jit(solution)/shard_map/layer/pallas_call | solution.py:667
  61.6 1.3 %copy.20 = bf16[64,64]{1,0:T(8,128)(2,1)} copy(bf16[64,64]{1,0:T(8,128)(2,1)} %layer.1) | data formatting | bytes 16384

commit v4 on v3

--- a/solution.py
+++ b/solution.py
@@ -61,19 +61,17 @@
     wmg,
     wmu,
     wmd,
-    x0,
-    x1,
-    ra0,
-    ra1,
-    rs0,
-    rs1,
-    rb0,
-    rb1,
+    xa,
+    xb,
+    xfa,
+    xfb,
+    xsa,
+    xsb,
+    xba,
+    xbb,
     zf,
-    zs0,
-    zs1,
-    zr0,
-    zr1,
+    zs,
+    zr,
     memory,
     pack0,
     pack1,
@@ -109,7 +107,7 @@
     dzsem,
 ):
     nz, qb, vb, dk, width = sizes
-    rows2 = 2 * nz
+    nh = nz // 2
     kv = lax.axis_index("kv")
     c = lax.axis_index("tp")
     other = 1 - c
@@ -122,6 +120,18 @@
     far = [(z + (s % nz)) % nz for s in steps][::-1]
     near = [(z + (s % nz)) % nz for s in steps]
     sides = [(x + d) % NX for d in (2, 1, 3)]
+    last = near[-1]
+
+    def turn(g, j):
+        return (nz // 4 + g * nh + j) % nz
+
+    def zrel(g, j):
+        return (z + turn(g, j)) % nz
+
+    def by_distance(g):
+        return sorted(range(nh), key=lambda j: -min(turn(g, j), nz - turn(g, j)))
+
+    self_g, self_j = divmod((nz - nz // 4) % nz, nh)
 
     def local(i, src, dst):
         copy = pltpu.make_async_copy(src, dst, lsem.at[i])
@@ -188,6 +198,7 @@
         greet(zp * NX + x, other)
     for xp in sides:
         greet(z * NX + xp, c)
+        greet(last * NX + xp, c)
     greet(kv, other)
     zf[...] = jnp.zeros_like(zf)
     for copy in in_small:
@@ -198,7 +209,7 @@
             hg[h * (vb // 2) + b : h * (vb // 2) + b + 1, :] = hgain[
                 h : h + 1, b * LANES : (b + 1) * LANES
             ].astype(F32)
-    pl.semaphore_wait(barrier, 2 * len(far) + len(sides) + 1)
+    pl.semaphore_wait(barrier, 2 * len(far) + 2 * len(sides) + 1)
 
     mark("tokens")
     in_tok.wait()
@@ -207,24 +218,29 @@
     send(wo.at[c], wo.at[c], psem.at[2], psem.at[3], kv, other)
     remote(tok.at[other], tok.at[other], psem.at[0], psem.at[1], kv, other).wait_recv()
     tokf[...] = jnp.concatenate([tok[0].astype(F32), tok[1].astype(F32)], axis=1)
-    block = jnp.concatenate(
-        [
-            tokf[pl.ds(2 * xp + i, nz, stride=2 * NX), :]
-            for xp in range(NX)
+    block = []
+    for xp in range(NX):
+        pair = [
+            pltpu.roll(
+                tokf[pl.ds(2 * xp + i, nz, stride=2 * NX), :], (2 * nz - z - nz // 4) % nz, 0
+            )
             for i in range(2)
-        ],
-        axis=0,
-    )
+        ]
+        for g in range(2):
+            block += [rows[g * nh : (g + 1) * nh] for rows in pair]
+    block = jnp.concatenate(block, axis=0)
     squares = jnp.sum(block * block, axis=1, keepdims=True)
     scaled = (block * again[...].astype(F32)).astype(BF16)
 
     def put(target, b, values):
-        half = target.shape[2] // LANES
+        half = target.shape[3] // LANES
         at = (b % half) * LANES
         for xp in range(NX):
-            target[2 * xp + b // half, :, at : at + LANES] = values[
-                xp * rows2 : (xp + 1) * rows2
-            ].astype(BF16)
+            for g in range(2):
+                row = (2 * xp + g) * nz
+                target[g, 2 * xp + b // half, :, at : at + LANES] = values[row : row + nz].astype(
+                    BF16
+                )
 
     def project(copy, weight, target, start):
         copy.wait()
@@ -238,6 +254,9 @@
         out_sem, in_left, in_right, in_back = [xsem.at[stage, k] for k in range(4)]
         send(src.at[2 * xo], first.at[0], out_sem, in_left, right, c)
         send(src.at[2 * xo + 1], first.at[1], out_sem, in_right, left, c)
+
+    def x_direct(src, first, back, stage):
+        out_sem, in_left, in_right, in_back = [xsem.at[stage, k] for k in range(4)]
         send(src.at[2 * xr + 1], back.at[1], out_sem, in_back, right, c)
         send(src.at[2 * xl], back.at[2], out_sem, in_back, left, c)
 
@@ -262,17 +281,33 @@
             src[2 * x + half].astype(F32) + back[half].astype(F32) + back[2 + half].astype(F32)
         )
 
-    project(in_w[0], wq, x0, 0)
-    project(in_w[1], wk, x0, qb)
-    project(in_w[2], wd, x0, 2 * qb)
-    put(x0, 3 * qb, jnp.broadcast_to(squares, (squares.shape[0], LANES)))
-    for b in range(3 * qb + 1, 2 * (x0.shape[2] // LANES)):
-        put(x0, b, jnp.zeros((squares.shape[0], LANES), F32))
-    x_first(x0, ra0, rb0, 0)
+    def x_stage(g, col):
+        src, first, relay, back = ((xa, xfa, xsa, xba), (xb, xfb, xsb, xbb))[col]
+        return src.at[g], first.at[g], relay.at[g], back.at[g], 2 * g + col
+
+    def x_one(g, col):
+        src, first, relay, back, stage = x_stage(g, col)
+        x_first(src, first, back, stage)
+
+    def x_ind(g, col):
+        src, first, relay, back, stage = x_stage(g, col)
+        x_direct(src, first, back, stage)
+
+    project(in_w[0], wq, xa, 0)
+    project(in_w[1], wk, xa, qb)
+    project(in_w[2], wd, xa, 2 * qb)
+    put(xa, 3 * qb, jnp.broadcast_to(squares, (squares.shape[0], LANES)))
+    for b in range(3 * qb + 1, 2 * (xa.shape[3] // LANES)):
+        put(xa, b, jnp.zeros((squares.shape[0], LANES), F32))
+    x_one(0, 0)
     mark("project_b")
-    project(in_w[3], wv, x1, 0)
-    project(in_w[4], wg, x1, vb)
-    x_first(x1, ra1, rb1, 1)
+    project(in_w[3], wv, xb, 0)
+    project(in_w[4], wg, xb, vb)
+    x_one(0, 1)
+    x_ind(0, 0)
+    x_ind(0, 1)
+    x_one(1, 0)
+    x_one(1, 1)
 
     span = ck.shape[2]
     hb = vb // 2
@@ -297,51 +332,73 @@
             cols = slice(b * LANES, (b + 1) * LANES)
             memory[i, h, :, cols] = (st[i, h, :, cols] * shrink + inner[:, cols]).astype(BF16)
 
-    mark("x_second")
+    mark("fold_a")
     for copy in in_cache:
         copy.wait()
     in_state.wait()
-    x_second(x0, ra0, rs0, rb0, 0)
-    x_second(x1, ra1, rs1, rb1, 1)
-
-    slots_row = zf.shape[0] // rows2
-
-    def z_send(src, back, packed, landing, stage):
+    for h in range(2):
+        fold(0, h)
+    mark("x_second_a")
+    x_second(*x_stage(0, 0))
+    x_second(*x_stage(0, 1))
+    mark("x_second_b")
+    x_ind(1, 0)
+    x_ind(1, 1)
+    x_second(*x_stage(1, 0))
+    x_second(*x_stage(1, 1))
+
+    slots_row = zf.shape[0] // (2 * nh)
+
+    def z_send(g, col):
+        src, first, relay, back, stage = x_stage(g, col)
         half = src.shape[2] // LANES
         x_wait(back, stage)
         for hh in (0, 1):
             total = x_sum(src, back, hh)
             for b in range(half):
                 for i in range(2):
-                    zf[pl.ds(i * slots_row + hh * half + b, nz, stride=2 * slots_row), :] = total[
-                        i * nz : (i + 1) * nz, b * LANES : (b + 1) * LANES
+                    zf[pl.ds(i * slots_row + hh * half + b, nh, stride=2 * slots_row), :] = total[
+                        i * nh : (i + 1) * nh, b * LANES : (b + 1) * LANES
                     ]
-        for zp in range(nz):
-            packed[zp] = zf[zp * 2 * slots_row : (zp + 1) * 2 * slots_row, :].astype(BF16)
-        for zp in far:
-            send(
-                packed.at[zp], landing.at[z], zsem.at[stage, 0], zsem.at[stage, 1], zp * NX + x, c
-            )
-
-    def z_sum(packed, landing, stage):
-        part = landing.at[pl.ds(0, nz - 1)]
-        remote(part, part, zsem.at[stage, 0], zsem.at[stage, 1], left, c).wait_recv()
-        total = packed[z].astype(F32)
-        for zp in near:
-            total = total + landing[zp].astype(F32)
+        for j in by_distance(g):
+            zs[stage, j] = zf[j * 2 * slots_row : (j + 1) * 2 * slots_row, :].astype(BF16)
+            if (g, j) != (self_g, self_j):
+                send(
+                    zs.at[stage, j],
+                    zr.at[stage, j],
+                    zsem.at[stage, 0],
+                    zsem.at[stage, 1],
+                    zrel(g, j) * NX + x,
+                    c,
+                )
+
+    def z_part(g, col):
+        return zr.at[2 * g + col, pl.ds(0, nh - (g == self_g))]
+
+    def z_sum(col):
+        for g in range(2):
+            part = z_part(g, col)
+            stage = 2 * g + col
+            remote(part, part, zsem.at[stage, 0], zsem.at[stage, 1], left, c).wait_recv()
+        total = zs[2 * self_g + col, self_j].astype(F32)
+        for g in range(2):
+            for j in range(nh):
+                if (g, j) != (self_g, self_j):
+                    total = total + zr[2 * g + col, j].astype(F32)
         return total
 
     mark("z_send_a")
-    z_send(x0, rb0, zs0, zr0, 0)
+    z_send(0, 0)
+    z_send(0, 1)
+    mark("fold_b")
+    for h in range(2):
+        fold(1, h)
     mark("z_send_b")
-    z_send(x1, rb1, zs1, zr1, 1)
-    mark("fold")
-    for i in range(2):
-        for h in range(2):
-            fold(i, h)
+    z_send(1, 0)
+    z_send(1, 1)
 
     mark("z_wait_a")
-    pack0[...] = z_sum(zs0, zr0, 0)
+    pack0[...] = z_sum(0)
     mark("heads_a")
     own = []
     inverse = []
@@ -372,7 +429,7 @@
                     :, b * LANES : (b + 1) * LANES
                 ]
     mark("z_wait_b")
-    pack1[...] = z_sum(zs1, zr1, 1)
+    pack1[...] = z_sum(1)
     for i in range(2):
         at = i * slots_row
         if i == 0:
@@ -394,35 +451,60 @@
     def gather(buf, sems, with_partner, consume):
         out_sem = sems.at[0]
         mine = buf.at[2 * kv + c]
+
+        def in_z(zp):
+            return sems.at[1 + zp]
+
+        def in_x(zp):
+            return sems.at[1 + nz + zp]
+
+        def in_peer(zp):
+            return sems.at[1 + 2 * nz + zp]
+
+        for xp in sides:
+            send(mine, mine, out_sem, in_x(z), last * NX + xp, c)
         for zp in far:
-            send(mine, mine, out_sem, sems.at[1 + z], zp * NX + x, c)
+            send(mine, mine, out_sem, in_z(z), zp * NX + x, c)
         for xp in sides:
-            send(mine, mine, out_sem, sems.at[1 + nz + z], z * NX + xp, c)
+            send(mine, mine, out_sem, in_x(z), z * NX + xp, c)
         if with_partner:
-            send(mine, mine, out_sem, sems.at[1 + 2 * nz + z], kv, other)
-        for zp in near:
+            send(mine, mine, out_sem, in_peer(z), kv, other)
+
+        def take_z(zp):
             origin = zp * NX + x
             slot = buf.at[2 * origin + c]
-            remote(slot, slot, out_sem, sems.at[1 + zp], origin, c).wait_recv()
-            for xp in sides:
-                send(slot, slot, out_sem, sems.at[1 + nz + zp], z * NX + xp, c)
-            send(slot, slot, out_sem, sems.at[1 + 2 * nz + zp], kv, other)
-        order = [z] + near
+            remote(slot, slot, out_sem, in_z(zp), origin, c).wait_recv()
+            if zp is not last:
+                for xp in sides:
+                    send(slot, slot, out_sem, in_x(zp), z * NX + xp, c)
+            send(slot, slot, out_sem, in_peer(zp), kv, other)
+
+        def take_x(zp):
+            part = buf.at[pl.ds(0, NX - 1)]
+            remote(part, part, out_sem, in_x(zp), left, c).wait_recv()
+            for xp in sides[::-1]:
+                slot = buf.at[2 * (zp * NX + xp) + c]
+                send(slot, slot, out_sem, in_peer(zp), kv, other)
 
         def finish(zp):
             part = buf.at[pl.ds(0, NX - (zp is z and not with_partner))]
-            remote(part, part, out_sem, sems.at[1 + 2 * nz + zp], kv, other).wait_recv()
+            remote(part, part, out_sem, in_peer(zp), kv, other).wait_recv()
             consume(zp)
 
+        for n, zp in enumerate(near):
+            take_z(zp)
+            if n == len(near) // 2:
+                take_x(z)
+        mark("take_x")
+        finish(z)
+        order = near[:-1][:4] + [last] + near[:-1][4:]
         for n, zp in enumerate(order):
-            part = buf.at[pl.ds(0, NX - 1)]
-            remote(part, part, out_sem, sems.at[1 + nz + zp], left, c).wait_recv()
-            for xp in sides[::-1]:
-                slot = buf.at[2 * (zp * NX + xp) + c]
-                send(slot, slot, out_sem, sems.at[1 + 2 * nz + zp], kv, other)
-            if n:
-                finish(order[n - 1])
-        finish(order[-1])
+            take_x(zp)
+            if n >= 3:
+                finish(order[n - 3])
+        mark("take_peer")
+        for zp in order[-min(3, len(order)) :]:
+            finish(zp)
 
     def gather_drain(buf, sems, with_partner):
         part = buf.at[pl.ds(0, 2 * nz * NX - 1 - (not with_partner))]
@@ -483,31 +565,36 @@
     hidden[...] = (gate / (1.0 + jnp.exp(-gate)) * up).astype(BF16)
     mark("mlp_down")
     in_mlp[2].wait()
-    hz_half = nz // 2
-    for zh in range(2):
-        for zi in range(hz_half):
-            zp = zh * hz_half + zi
-            part = dot(hidden[...], wmd[:, zp * NX * LANES : (zp + 1) * NX * LANES]).astype(BF16)
+    for g in range(2):
+        for j in range(nh):
+            cols = pl.ds(pl.multiple_of(zrel(g, j) * NX * LANES, LANES), NX * LANES)
+            part = dot(hidden[...], wmd[:, cols]).astype(BF16)
             for xp in range(NX):
-                for i in range(2):
-                    dpart[i, zh, xp, :, zi * LANES : (zi + 1) * LANES] = part[
-                        i * n_kv : (i + 1) * n_kv, xp * LANES : (xp + 1) * LANES
+                for k in range(4):
+                    dpart[k // 2, g, 2 * xp + k % 2, :, j * LANES : (j + 1) * LANES] = part[
+                        k * n_kv // 2 : (k + 1) * n_kv // 2, xp * LANES : (xp + 1) * LANES
                     ]
-        send(dpart.at[other, zh], dpeer.at[zh], psem.at[4], psem.at[5 + zh], kv, other)
+        send(dpart.at[other, g], dpeer.at[g], psem.at[4], psem.at[5 + g], kv, other)
     mark("down_peer")
-    for zh in range(2):
-        remote(
-            dpeer.at[zh], dpeer.at[zh], psem.at[4], psem.at[5 + zh], kv, other
-        ).wait_recv()
+
+    def d_stage(g):
+        return dx.at[g], dra.at[g], drs.at[g], drb.at[g], 4 + g
+
+    for g in range(2):
+        remote(dpeer.at[g], dpeer.at[g], psem.at[4], psem.at[5 + g], kv, other).wait_recv()
         for xp in (xo, xr, xl, x):
-            dx[2 * xp + zh] = (dpart[c, zh, xp].astype(F32) + dpeer[zh, xp].astype(F32)).astype(BF16)
+            for k in range(2):
+                dx[g, 2 * xp + k] = (
+                    dpart[c, g, 2 * xp + k].astype(F32) + dpeer[g, 2 * xp + k].astype(F32)
+                ).astype(BF16)
+        x_first(dx.at[g], dra.at[g], drb.at[g], 4 + g)
+        x_direct(dx.at[g], dra.at[g], drb.at[g], 4 + g)
     mark("down_x")
-    x_first(dx, dra, drb, 2)
-    x_second(dx, dra, drs, drb, 2)
+    for g in range(2):
+        x_second(*d_stage(g))
     low_lanes = lax.broadcasted_iota(jnp.int32, (n_kv // 2, LANES), 1) < LANES // 2
 
-    def squeeze(rows, right):
-        top, bottom = rows[: n_kv // 2], rows[n_kv // 2 :]
+    def squeeze(top, bottom, right):
         if right:
             top = pltpu.roll(top, LANES // 2, 1)
         else:
@@ -515,33 +602,35 @@
         return jnp.where(low_lanes, top, bottom)
 
     mark("down_x2")
-    x_wait(drb, 2)
-    mark("down_pack")
-    for zh in range(2):
-        total = x_sum(dx, drb, zh)
-        for zi in range(hz_half):
-            rows = total[:, zi * LANES : (zi + 1) * LANES]
+    for g in range(2):
+        x_wait(drb.at[g], 4 + g)
+        top, bottom = [x_sum(dx.at[g], drb.at[g], k) for k in range(2)]
+        for j in by_distance(g):
+            cols = slice(j * LANES, (j + 1) * LANES)
+            slot = 2 * (g * nh + j)
             for cc in range(2):
-                dzs[2 * (zh * hz_half + zi) + cc] = squeeze(rows, cc == 1).astype(BF16)
-    for zp in far:
-        for cc in (other, c):
-            send(
-                dzs.at[2 * zp + cc],
-                dzr.at[2 * z + c],
-                dzsem.at[0],
-                dzsem.at[1],
-                zp * NX + x,
-                cc,
-            )
-    send(dzs.at[2 * z + other], dzr.at[2 * z + c], dzsem.at[0], dzsem.at[1], kv, other)
-    dzr[2 * z + c] = dzs[2 * z + c]
+                dzs[slot + cc] = squeeze(top[:, cols], bottom[:, cols], cc == 1).astype(BF16)
+            if (g, j) == (self_g, self_j):
+                dzr[slot + c] = dzs[slot + c]
+                send(dzs.at[slot + other], dzr.at[slot + c], dzsem.at[0], dzsem.at[1], kv, other)
+            else:
+                for cc in (other, c):
+                    send(
+                        dzs.at[slot + cc],
+                        dzr.at[slot + c],
+                        dzsem.at[0],
+                        dzsem.at[1],
+                        zrel(g, j) * NX + x,
+                        cc,
+                    )
     mark("down_z")
     part = dzr.at[pl.ds(0, 2 * nz - 1)]
     remote(part, part, dzsem.at[0], dzsem.at[1], kv, other).wait_recv()
     mark("finish")
     for i in range(2):
         rows = whole[2 * kv + i].astype(F32)
-        total = jnp.where(c == 1, squeeze(rows, True), squeeze(rows, False))
+        halves = rows[: n_kv // 2], rows[n_kv // 2 :]
+        total = jnp.where(c == 1, squeeze(*halves, True), squeeze(*halves, False))
         for zp in range(nz):
             total = total + dzr[2 * zp + i].astype(F32)
         outf[pl.ds(i, n_kv // 2, stride=2), :] = total
@@ -550,15 +639,16 @@
     mark("drain")
     remote(tok.at[c], tok.at[c], psem.at[0], psem.at[1], kv, other).wait_send()
     remote(wo.at[c], wo.at[c], psem.at[2], psem.at[3], kv, other).wait_send()
-    x_drain(x0, 0)
-    x_drain(x1, 1)
-    for stage, landing in enumerate((zr0, zr1)):
-        part = landing.at[pl.ds(0, nz - 1)]
-        remote(part, part, zsem.at[stage, 0], zsem.at[stage, 1], left, c).wait_send()
+    for g in range(2):
+        for col in range(2):
+            stage = 2 * g + col
+            x_drain((xa, xb)[col].at[g], stage)
+            part = z_part(g, col)
+            remote(part, part, zsem.at[stage, 0], zsem.at[stage, 1], left, c).wait_send()
+        x_drain(dx.at[g], 4 + g)
     gather_drain(headb, hsem, True)
     gather_drain(whole, asem, False)
     remote(dpeer, dpeer, psem.at[4], psem.at[5], kv, other).wait_send()
-    x_drain(dx, 2)
     part = dzr.at[pl.ds(0, 2 * nz - 1)]
     remote(part, part, dzsem.at[0], dzsem.at[1], kv, other).wait_send()
     mark()
@@ -591,11 +681,11 @@
     qb, vb = heads * dk // LANES, heads * dv // LANES
     half0, half1 = (3 * qb + 2) // 2, vb
     slots = -(-2 * max(half0, half1) // 8) * 8
-    rows2 = 2 * nz
+    nh = nz // 2
     seqs = 2 * n_kv
     hrows = 2 * vb
     units = w_mlp_down.shape[0]
-    cols5 = nz // 2 * LANES
+    cols5 = nh * LANES
     vmem, dma = pltpu.VMEM, pltpu.SemaphoreType.DMA
     bf, fl = BF16, F32
     scratch = [
@@ -614,19 +704,17 @@
         vmem(w_mlp_gate.shape[::-1], bf),
         vmem(w_mlp_up.shape[::-1], bf),
         vmem(w_mlp_down.shape, bf),
-        vmem((NX * 2, rows2, half0 * LANES), bf),
-        vmem((NX * 2, rows2, half1 * LANES), bf),
-        vmem((2, rows2, half0 * LANES), bf),
-        vmem((2, rows2, half1 * LANES), bf),
-        vmem((2, rows2, half0 * LANES), bf),
-        vmem((2, rows2, half1 * LANES), bf),
-        vmem((4, rows2, half0 * LANES), bf),
-        vmem((4, rows2, half1 * LANES), bf),
-        vmem((rows2 * slots, LANES), fl),
-        vmem((nz, 2 * slots, LANES), bf),
-        vmem((nz, 2 * slots, LANES), bf),
-        vmem((nz, 2 * slots, LANES), bf),
-        vmem((nz, 2 * slots, LANES), bf),
+        vmem((2, NX * 2, nz, half0 * LANES), bf),
+        vmem((2, NX * 2, nz, half1 * LANES), bf),
+        vmem((2, 2, nz, half0 * LANES), bf),
+        vmem((2, 2, nz, half1 * LANES), bf),
+        vmem((2, 2, nz, half0 * LANES), bf),
+        vmem((2, 2, nz, half1 * LANES), bf),
+        vmem((2, 4, nz, half0 * LANES), bf),
+        vmem((2, 4, nz, half1 * LANES), bf),
+        vmem((nz * slots, LANES), fl),
+        vmem((4, nh, 2 * slots, LANES), bf),
+        vmem((4, nh, 2 * slots, LANES), bf),
         vmem(state.shape, bf),
         vmem((2 * slots, LANES), fl),
         vmem((2 * slots, LANES), fl),
@@ -639,12 +727,12 @@
         vmem((seqs, 2 * vb * LANES), bf),
         vmem((2 * n_kv, n_kv, LANES), bf),
         vmem((seqs, units), bf),
-        vmem((2, 2, NX, n_kv, cols5), bf),
-        vmem((2, NX, n_kv, cols5), bf),
-        vmem((NX * 2, n_kv, cols5), bf),
-        vmem((2, n_kv, cols5), bf),
-        vmem((2, n_kv, cols5), bf),
-        vmem((4, n_kv, cols5), bf),
+        vmem((2, 2, NX * 2, n_kv // 2, cols5), bf),
+        vmem((2, NX * 2, n_kv // 2, cols5), bf),
+        vmem((2, NX * 2, n_kv // 2, cols5), bf),
+        vmem((2, 2, n_kv // 2, cols5), bf),
+        vmem((2, 2, n_kv // 2, cols5), bf),
+        vmem((2, 4, n_kv // 2, cols5), bf),
         vmem((2 * nz, n_kv // 2, LANES), bf),
         vmem((2 * nz, n_kv // 2, LANES), bf),
         vmem((seqs, LANES), fl),
@@ -655,8 +743,8 @@
         pltpu.SMEM((2,), jnp.int32),
         dma((18,)),
         dma((7,)),
-        dma((3, 4)),
-        dma((2, 2)),
+        dma((6, 4)),
+        dma((4, 2)),
         dma((1 + 3 * nz,)),
         dma((1 + 3 * nz,)),
         dma((2,)),

time: 63 us -> 60.4 us (0.959)
  Pallas kernels: 61.5 us -> 58.9 us
    pallas_call x1, Pallas kernels: 61.5 us -> 58.9 us  [shards(): pl.pallas_call(functools.partial(kernel, (nz, qb, vb, dk, width)), out_sh...]
where the time goes in v4:
time: 60.4 us; the launch traced here: 60.2 us
  Pallas kernels  58.9 us (98%)
  local copies, waits for them, and re-layouts  1.32 us (2%)
    pallas_call x1, Pallas kernels, shards(): pl.pallas_call(functools.partial(kernel, (nz, qb, vb, dk, width)), out_sh...  58.9 us
    unnamed x1, local copies, waits for them, and re-layouts  1.32 us

profile of v4, /device:TPU:1, one launch (start us, length us, event | category | flops | bytes accessed | tf_op | source)
XLA Modules:
  0.0 60.2 jit_solution(10274923613943668757)
XLA Ops:
  0.0 58.9 %layer.1 = bf16[64,64]{1,0:T(8,128)(2,1)} custom-call(bf16[64,64]{1,0:T(8,128)(2,1)} %tokens.1, s32[2]{0:T(128)} %lengths.1, f32[2,2,384,768]{3,2,1,0:T(8,128)} %state.1, bf16[2,2,64,384]{3,2,1,0:T(8,128)(2,1)} %cache_keys.1, bf16[2,2,64,768]{3,2,1,0:T(8,128)(2,1)} %cache_values.1, f32[2,2,64,384]{3,2,1,0:T(8,128)} %cache_rates.1, bf16[1,128]{1,0:T(2,128)(2,1)} %bitcast.9, ...), custom_call_target="tpu_custom_call" | custom-call | tf_op jit(solution)/shard_map/layer/pallas_call | solution.py:755
  58.9 1.3 %copy.20 = bf16[64,64]{1,0:T(8,128)(2,1)} copy(bf16[64,64]{1,0:T(8,128)(2,1)} %layer.1) | data formatting | bytes 16384

commit v5 on v4

--- a/solution.py
+++ b/solution.py
@@ -87,8 +87,6 @@
     dpart,
     dpeer,
     dx,
-    dra,
-    drs,
     drb,
     dzs,
     dzr,
@@ -104,6 +102,7 @@
     zsem,
     hsem,
     asem,
+    dxsem,
     dzsem,
 ):
     nz, qb, vb, dk, width = sizes
@@ -120,7 +119,6 @@
     far = [(z + (s % nz)) % nz for s in steps][::-1]
     near = [(z + (s % nz)) % nz for s in steps]
     sides = [(x + d) % NX for d in (2, 1, 3)]
-    last = near[-1]
 
     def turn(g, j):
         return (nz // 4 + g * nh + j) % nz
@@ -160,6 +158,20 @@
     def send(*args):
         remote(*args).start()
 
+    mark("barrier")
+    barrier = pltpu.get_barrier_semaphore()
+
+    def greet(to_kv, to_tp):
+        pl.semaphore_signal(
+            barrier, inc=1, device_id={"kv": to_kv, "tp": to_tp}, device_id_type=MESH
+        )
+
+    for zp in far:
+        greet(zp * NX + x, c)
+        greet(zp * NX + x, other)
+    for xp in sides:
+        greet(z * NX + xp, c)
+    greet(kv, other)
     mark("load")
     in_tok = local(0, tokens, tok.at[c])
     in_small = [
@@ -185,31 +197,8 @@
         for i, (src, dst) in enumerate(((w_mlp_gate, wmg), (w_mlp_up, wmu), (w_mlp_down, wmd)))
     ]
 
-    mark("barrier")
-    barrier = pltpu.get_barrier_semaphore()
-
-    def greet(to_kv, to_tp):
-        pl.semaphore_signal(
-            barrier, inc=1, device_id={"kv": to_kv, "tp": to_tp}, device_id_type=MESH
-        )
-
-    for zp in far:
-        greet(zp * NX + x, c)
-        greet(zp * NX + x, other)
-    for xp in sides:
-        greet(z * NX + xp, c)
-        greet(last * NX + xp, c)
-    greet(kv, other)
     zf[...] = jnp.zeros_like(zf)
-    for copy in in_small:
-        copy.wait()
-    mgainf[...] = mgain[...].astype(F32)
-    for h in range(2):
-        for b in range(vb // 2):
-            hg[h * (vb // 2) + b : h * (vb // 2) + b + 1, :] = hgain[
-                h : h + 1, b * LANES : (b + 1) * LANES
-            ].astype(F32)
-    pl.semaphore_wait(barrier, 2 * len(far) + 2 * len(sides) + 1)
+    pl.semaphore_wait(barrier, 2 * len(far) + len(sides) + 1)
 
     mark("tokens")
     in_tok.wait()
@@ -229,6 +218,7 @@
         for g in range(2):
             block += [rows[g * nh : (g + 1) * nh] for rows in pair]
     block = jnp.concatenate(block, axis=0)
+    in_small[0].wait()
     squares = jnp.sum(block * block, axis=1, keepdims=True)
     scaled = (block * again[...].astype(F32)).astype(BF16)
 
@@ -333,6 +323,14 @@
             memory[i, h, :, cols] = (st[i, h, :, cols] * shrink + inner[:, cols]).astype(BF16)
 
     mark("fold_a")
+    for copy in in_small[1:]:
+        copy.wait()
+    mgainf[...] = mgain[...].astype(F32)
+    for h in range(2):
+        for b in range(hb):
+            hg[h * hb + b : h * hb + b + 1, :] = hgain[
+                h : h + 1, b * LANES : (b + 1) * LANES
+            ].astype(F32)
     for copy in in_cache:
         copy.wait()
     in_state.wait()
@@ -461,8 +459,6 @@
         def in_peer(zp):
             return sems.at[1 + 2 * nz + zp]
 
-        for xp in sides:
-            send(mine, mine, out_sem, in_x(z), last * NX + xp, c)
         for zp in far:
             send(mine, mine, out_sem, in_z(z), zp * NX + x, c)
         for xp in sides:
@@ -474,9 +470,8 @@
             origin = zp * NX + x
             slot = buf.at[2 * origin + c]
             remote(slot, slot, out_sem, in_z(zp), origin, c).wait_recv()
-            if zp is not last:
-                for xp in sides:
-                    send(slot, slot, out_sem, in_x(zp), z * NX + xp, c)
+            for xp in sides:
+                send(slot, slot, out_sem, in_x(zp), z * NX + xp, c)
             send(slot, slot, out_sem, in_peer(zp), kv, other)
 
         def take_x(zp):
@@ -491,19 +486,19 @@
             remote(part, part, out_sem, in_peer(zp), kv, other).wait_recv()
             consume(zp)
 
-        for n, zp in enumerate(near):
+        for zp in near:
             take_z(zp)
-            if n == len(near) // 2:
-                take_x(z)
         mark("take_x")
+        split = (len(near) + 1) // 2
+        for zp in [z] + near[:split]:
+            take_x(zp)
         finish(z)
-        order = near[:-1][:4] + [last] + near[:-1][4:]
-        for n, zp in enumerate(order):
+        for zp in near[: split // 2]:
+            finish(zp)
+        for zp in near[split:]:
             take_x(zp)
-            if n >= 3:
-                finish(order[n - 3])
         mark("take_peer")
-        for zp in order[-min(3, len(order)) :]:
+        for zp in near[split // 2 :]:
             finish(zp)
 
     def gather_drain(buf, sems, with_partner):
@@ -577,21 +572,22 @@
         send(dpart.at[other, g], dpeer.at[g], psem.at[4], psem.at[5 + g], kv, other)
     mark("down_peer")
 
-    def d_stage(g):
-        return dx.at[g], dra.at[g], drs.at[g], drb.at[g], 4 + g
-
     for g in range(2):
         remote(dpeer.at[g], dpeer.at[g], psem.at[4], psem.at[5 + g], kv, other).wait_recv()
-        for xp in (xo, xr, xl, x):
+        for n, xp in enumerate(sides + [x]):
             for k in range(2):
                 dx[g, 2 * xp + k] = (
                     dpart[c, g, 2 * xp + k].astype(F32) + dpeer[g, 2 * xp + k].astype(F32)
                 ).astype(BF16)
-        x_first(dx.at[g], dra.at[g], drb.at[g], 4 + g)
-        x_direct(dx.at[g], dra.at[g], drb.at[g], 4 + g)
-    mark("down_x")
-    for g in range(2):
-        x_second(*d_stage(g))
+            if n < NX - 1:
+                send(
+                    dx.at[g, pl.ds(2 * xp, 2)],
+                    drb.at[g, pl.ds(2 * n, 2)],
+                    dxsem.at[g, 0],
+                    dxsem.at[g, 1],
+                    z * NX + xp,
+                    c,
+                )
     low_lanes = lax.broadcasted_iota(jnp.int32, (n_kv // 2, LANES), 1) < LANES // 2
 
     def squeeze(top, bottom, right):
@@ -603,8 +599,13 @@
 
     mark("down_x2")
     for g in range(2):
-        x_wait(drb.at[g], 4 + g)
-        top, bottom = [x_sum(dx.at[g], drb.at[g], k) for k in range(2)]
+        part = drb.at[g]
+        remote(part, part, dxsem.at[g, 0], dxsem.at[g, 1], left, c).wait_recv()
+        top, bottom = [
+            dx[g, 2 * x + k].astype(F32)
+            + sum(drb[g, 2 * n + k].astype(F32) for n in range(NX - 1))
+            for k in range(2)
+        ]
         for j in by_distance(g):
             cols = slice(j * LANES, (j + 1) * LANES)
             slot = 2 * (g * nh + j)
@@ -645,7 +646,8 @@
             x_drain((xa, xb)[col].at[g], stage)
             part = z_part(g, col)
             remote(part, part, zsem.at[stage, 0], zsem.at[stage, 1], left, c).wait_send()
-        x_drain(dx.at[g], 4 + g)
+        part = drb.at[g]
+        remote(part, part, dxsem.at[g, 0], dxsem.at[g, 1], left, c).wait_send()
     gather_drain(headb, hsem, True)
     gather_drain(whole, asem, False)
     remote(dpeer, dpeer, psem.at[4], psem.at[5], kv, other).wait_send()
@@ -730,9 +732,7 @@
         vmem((2, 2, NX * 2, n_kv // 2, cols5), bf),
         vmem((2, NX * 2, n_kv // 2, cols5), bf),
         vmem((2, NX * 2, n_kv // 2, cols5), bf),
-        vmem((2, 2, n_kv // 2, cols5), bf),
-        vmem((2, 2, n_kv // 2, cols5), bf),
-        vmem((2, 4, n_kv // 2, cols5), bf),
+        vmem((2, 2 * (NX - 1), n_kv // 2, cols5), bf),
         vmem((2 * nz, n_kv // 2, LANES), bf),
         vmem((2 * nz, n_kv // 2, LANES), bf),
         vmem((seqs, LANES), fl),
@@ -743,10 +743,11 @@
         pltpu.SMEM((2,), jnp.int32),
         dma((18,)),
         dma((7,)),
-        dma((6, 4)),
+        dma((4, 4)),
         dma((4, 2)),
         dma((1 + 3 * nz,)),
         dma((1 + 3 * nz,)),
+        dma((2, 2)),
         dma((2,)),
     ]
     anywhere = pl.BlockSpec(memory_space=pl.ANY)

time: 60.4 us -> 58.1 us (0.962)
  Pallas kernels: 58.9 us -> 56.6 us
    pallas_call x1, Pallas kernels: 58.9 us -> 56.6 us  [shards(): pl.pallas_call(functools.partial(kernel, (nz, qb, vb, dk, width)), out_sh...]
where the time goes in v5:
time: 58.1 us; the launch traced here: 58 us
  Pallas kernels  56.6 us (97%)
  local copies, waits for them, and re-layouts  1.32 us (2%)
    pallas_call x1, Pallas kernels, shards(): pl.pallas_call(functools.partial(kernel, (nz, qb, vb, dk, width)), out_sh...  56.6 us
    unnamed x1, local copies, waits for them, and re-layouts  1.32 us

profile of v5, /device:TPU:1, one launch (start us, length us, event | category | flops | bytes accessed | tf_op | source)
XLA Modules:
  0.0 58.0 jit_solution(16412651301740573145)
XLA Ops:
  0.0 56.6 %layer.1 = bf16[64,64]{1,0:T(8,128)(2,1)} custom-call(bf16[64,64]{1,0:T(8,128)(2,1)} %tokens.1, s32[2]{0:T(128)} %lengths.1, f32[2,2,384,768]{3,2,1,0:T(8,128)} %state.1, bf16[2,2,64,384]{3,2,1,0:T(8,128)(2,1)} %cache_keys.1, bf16[2,2,64,768]{3,2,1,0:T(8,128)(2,1)} %cache_values.1, f32[2,2,64,384]{3,2,1,0:T(8,128)} %cache_rates.1, bf16[1,128]{1,0:T(2,128)(2,1)} %bitcast.9, ...), custom_call_target="tpu_custom_call" | custom-call | tf_op jit(solution)/shard_map/layer/pallas_call | solution.py:756
  56.6 1.3 %copy.20 = bf16[64,64]{1,0:T(8,128)(2,1)} copy(bf16[64,64]{1,0:T(8,128)(2,1)} %layer.1) | data formatting | bytes 16384

commit v6 on v5

--- a/solution.py
+++ b/solution.py
@@ -104,6 +104,7 @@
     asem,
     dxsem,
     dzsem,
+    csem,
 ):
     nz, qb, vb, dk, width = sizes
     nh = nz // 2
@@ -166,10 +167,11 @@
             barrier, inc=1, device_id={"kv": to_kv, "tp": to_tp}, device_id_type=MESH
         )
 
-    for zp in far:
+    up, down = (z + 1) % nz, (z + nz - 1) % nz
+    beside = [up, down][: nz - 1]
+    for zp in beside:
         greet(zp * NX + x, c)
-        greet(zp * NX + x, other)
-    for xp in sides:
+    for xp in (xr, xl):
         greet(z * NX + xp, c)
     greet(kv, other)
     mark("load")
@@ -197,8 +199,28 @@
         for i, (src, dst) in enumerate(((w_mlp_gate, wmg), (w_mlp_up, wmu), (w_mlp_down, wmd)))
     ]
 
-    zf[...] = jnp.zeros_like(zf)
-    pl.semaphore_wait(barrier, 2 * len(far) + len(sides) + 1)
+    mark("meet")
+    pl.semaphore_wait(barrier, len(beside) + 3)
+
+    rounds = nz // 2 - 1
+
+    def chain_send(r):
+        if r < rounds:
+            device = {"kv": up * NX + x, "tp": c}
+            pl.semaphore_signal(csem.at[2 * r], inc=1, device_id=device, device_id_type=MESH)
+            if r + 2 <= (nz - 1) // 2:
+                device = {"kv": down * NX + x, "tp": c}
+                pl.semaphore_signal(
+                    csem.at[2 * r + 1], inc=1, device_id=device, device_id_type=MESH
+                )
+
+    def chain_wait(r):
+        if r < rounds:
+            pl.semaphore_wait(csem.at[2 * r], 1)
+            if r + 2 <= (nz - 1) // 2:
+                pl.semaphore_wait(csem.at[2 * r + 1], 1)
+
+    chain_send(0)
 
     mark("tokens")
     in_tok.wait()
@@ -290,6 +312,8 @@
     for b in range(3 * qb + 1, 2 * (xa.shape[3] // LANES)):
         put(xa, b, jnp.zeros((squares.shape[0], LANES), F32))
     x_one(0, 0)
+    chain_wait(0)
+    chain_send(1)
     mark("project_b")
     project(in_w[3], wv, xb, 0)
     project(in_w[4], wg, xb, vb)
@@ -323,6 +347,7 @@
             memory[i, h, :, cols] = (st[i, h, :, cols] * shrink + inner[:, cols]).astype(BF16)
 
     mark("fold_a")
+    zf[...] = jnp.zeros_like(zf)
     for copy in in_small[1:]:
         copy.wait()
     mgainf[...] = mgain[...].astype(F32)
@@ -336,6 +361,8 @@
     in_state.wait()
     for h in range(2):
         fold(0, h)
+    chain_wait(1)
+    chain_send(2)
     mark("x_second_a")
     x_second(*x_stage(0, 0))
     x_second(*x_stage(0, 1))
@@ -385,6 +412,7 @@
                     total = total + zr[2 * g + col, j].astype(F32)
         return total
 
+    chain_wait(2)
     mark("z_send_a")
     z_send(0, 0)
     z_send(0, 1)
@@ -749,6 +777,7 @@
         dma((1 + 3 * nz,)),
         dma((2, 2)),
         dma((2,)),
+        pltpu.SemaphoreType.REGULAR((max(1, 2 * (nz // 2) - 3),)),
     ]
     anywhere = pl.BlockSpec(memory_space=pl.ANY)
     in_vmem = pl.BlockSpec(memory_space=pltpu.VMEM)

time: 58.1 us -> 56.6 us (0.974)
  Pallas kernels: 56.6 us -> 55 us
    pallas_call x1, Pallas kernels: 56.6 us -> 55 us  [shards(): pl.pallas_call(functools.partial(kernel, (nz, qb, vb, dk, width)), out_sh...]
where the time goes in v6:
time: 56.6 us; the launch traced here: 56.3 us
  Pallas kernels  55 us (97%)
  local copies, waits for them, and re-layouts  1.32 us (2%)
    pallas_call x1, Pallas kernels, shards(): pl.pallas_call(functools.partial(kernel, (nz, qb, vb, dk, width)), out_sh...  55 us
    unnamed x1, local copies, waits for them, and re-layouts  1.32 us

profile of v6, /device:TPU:1, one launch (start us, length us, event | category | flops | bytes accessed | tf_op | source)
XLA Modules:
  0.0 56.3 jit_solution(15907602976651559708)
XLA Ops:
  0.0 55.0 %layer.1 = bf16[64,64]{1,0:T(8,128)(2,1)} custom-call(bf16[64,64]{1,0:T(8,128)(2,1)} %tokens.1, s32[2]{0:T(128)} %lengths.1, f32[2,2,384,768]{3,2,1,0:T(8,128)} %state.1, bf16[2,2,64,384]{3,2,1,0:T(8,128)(2,1)} %cache_keys.1, bf16[2,2,64,768]{3,2,1,0:T(8,128)(2,1)} %cache_values.1, f32[2,2,64,384]{3,2,1,0:T(8,128)} %cache_rates.1, bf16[1,128]{1,0:T(2,128)(2,1)} %bitcast.9, ...), custom_call_target="tpu_custom_call" | custom-call | tf_op jit(solution)/shard_map/layer/pallas_call | solution.py:785
  55.0 1.3 %copy.20 = bf16[64,64]{1,0:T(8,128)(2,1)} copy(bf16[64,64]{1,0:T(8,128)(2,1)} %layer.1) | data formatting | bytes 16384

commit v7 on v6

--- a/solution.py
+++ b/solution.py
@@ -58,9 +58,7 @@
     cv,
     cr,
     wo,
-    wmg,
-    wmu,
-    wmd,
+    wm,
     xa,
     xb,
     xfa,
@@ -84,8 +82,8 @@
     lhs,
     whole,
     hidden,
-    dpart,
-    dpeer,
+    partial,
+    kept,
     dx,
     drb,
     dzs,
@@ -177,7 +175,7 @@
     mark("load")
     in_tok = local(0, tokens, tok.at[c])
     in_small = [
-        local(14 + i, src, dst)
+        local(12 + i, src, dst)
         for i, (src, dst) in enumerate(
             ((attn_gain, again), (head_gain, hgain), (mlp_gain, mgain), (lengths, lens))
         )
@@ -195,9 +193,11 @@
     in_state = local(9, state, st)
     in_out = local(10, w_out, wo.at[c])
     in_mlp = [
-        local(11 + i, src, dst)
-        for i, (src, dst) in enumerate(((w_mlp_gate, wmg), (w_mlp_up, wmu), (w_mlp_down, wmd)))
+        pltpu.make_async_copy(src, wm.at[c, i], lsem.at[11])
+        for i, src in enumerate((w_mlp_gate, w_mlp_up, w_mlp_down))
     ]
+    for copy in in_mlp:
+        copy.start()
 
     mark("meet")
     pl.semaphore_wait(barrier, len(beside) + 3)
@@ -225,8 +225,6 @@
     mark("tokens")
     in_tok.wait()
     send(tok.at[c], tok.at[c], psem.at[0], psem.at[1], kv, other)
-    in_out.wait()
-    send(wo.at[c], wo.at[c], psem.at[2], psem.at[3], kv, other)
     remote(tok.at[other], tok.at[other], psem.at[0], psem.at[1], kv, other).wait_recv()
     tokf[...] = jnp.concatenate([tok[0].astype(F32), tok[1].astype(F32)], axis=1)
     block = []
@@ -312,8 +310,6 @@
     for b in range(3 * qb + 1, 2 * (xa.shape[3] // LANES)):
         put(xa, b, jnp.zeros((squares.shape[0], LANES), F32))
     x_one(0, 0)
-    chain_wait(0)
-    chain_send(1)
     mark("project_b")
     project(in_w[3], wv, xb, 0)
     project(in_w[4], wg, xb, vb)
@@ -347,6 +343,10 @@
             memory[i, h, :, cols] = (st[i, h, :, cols] * shrink + inner[:, cols]).astype(BF16)
 
     mark("fold_a")
+    chain_wait(0)
+    chain_send(1)
+    in_out.wait()
+    send(wo.at[c], wo.at[c], psem.at[2], psem.at[3], kv, other)
     zf[...] = jnp.zeros_like(zf)
     for copy in in_small[1:]:
         copy.wait()
@@ -423,6 +423,10 @@
     z_send(1, 0)
     z_send(1, 1)
 
+    mark("share")
+    pltpu.make_async_copy(wm.at[c], wm.at[c], lsem.at[11]).wait()
+    for k in range(3):
+        send(wm.at[c, k], wm.at[c, k], psem.at[6], psem.at[7], kv, other)
     mark("z_wait_a")
     pack0[...] = z_sum(0)
     mark("heads_a")
@@ -472,150 +476,115 @@
             headf[i * (headf.shape[0] // 2) + h * hb : i * (headf.shape[0] // 2) + (h + 1) * hb, :] = (
                 g / (1.0 + jnp.exp(-g)) * norm
             )
-    headb[2 * kv + c] = headf[...].astype(BF16)
-
-    def gather(buf, sems, with_partner, consume):
+    headb[kv] = headf[...].astype(BF16)
+
+    def gather(buf, sems, consume):
         out_sem = sems.at[0]
-        mine = buf.at[2 * kv + c]
+        mine = buf.at[kv]
 
         def in_z(zp):
             return sems.at[1 + zp]
 
         def in_x(zp):
             return sems.at[1 + nz + zp]
-
-        def in_peer(zp):
-            return sems.at[1 + 2 * nz + zp]
 
         for zp in far:
             send(mine, mine, out_sem, in_z(z), zp * NX + x, c)
         for xp in sides:
             send(mine, mine, out_sem, in_x(z), z * NX + xp, c)
-        if with_partner:
-            send(mine, mine, out_sem, in_peer(z), kv, other)
-
-        def take_z(zp):
-            origin = zp * NX + x
-            slot = buf.at[2 * origin + c]
-            remote(slot, slot, out_sem, in_z(zp), origin, c).wait_recv()
+        for zp in near:
+            slot = buf.at[zp * NX + x]
+            remote(slot, slot, out_sem, in_z(zp), zp * NX + x, c).wait_recv()
             for xp in sides:
                 send(slot, slot, out_sem, in_x(zp), z * NX + xp, c)
-            send(slot, slot, out_sem, in_peer(zp), kv, other)
-
-        def take_x(zp):
+        mark("take_x")
+        for zp in [z] + near:
             part = buf.at[pl.ds(0, NX - 1)]
             remote(part, part, out_sem, in_x(zp), left, c).wait_recv()
-            for xp in sides[::-1]:
-                slot = buf.at[2 * (zp * NX + xp) + c]
-                send(slot, slot, out_sem, in_peer(zp), kv, other)
-
-        def finish(zp):
-            part = buf.at[pl.ds(0, NX - (zp is z and not with_partner))]
-            remote(part, part, out_sem, in_peer(zp), kv, other).wait_recv()
             consume(zp)
 
-        for zp in near:
-            take_z(zp)
-        mark("take_x")
-        split = (len(near) + 1) // 2
-        for zp in [z] + near[:split]:
-            take_x(zp)
-        finish(z)
-        for zp in near[: split // 2]:
-            finish(zp)
-        for zp in near[split:]:
-            take_x(zp)
-        mark("take_peer")
-        for zp in near[split // 2 :]:
-            finish(zp)
-
-    def gather_drain(buf, sems, with_partner):
-        part = buf.at[pl.ds(0, 2 * nz * NX - 1 - (not with_partner))]
+    def gather_drain(buf, sems):
+        part = buf.at[pl.ds(0, nz * NX - 1)]
         remote(part, part, sems.at[0], sems.at[1], left, c).wait_send()
 
     n_kv = nz * NX
     hrows = headf.shape[0]
 
     def widen(zp):
-        for k in range(2 * NX):
-            slot = 2 * NX * zp + k
+        for k in range(NX):
+            slot = NX * zp + k
             headsf[pl.ds(pl.multiple_of(slot * hrows, 8), hrows), :] = headb[slot].astype(F32)
 
     mark("gather_heads")
-    gather(headb, hsem, True, widen)
+    gather(headb, hsem, widen)
 
     mark("project_out")
-    for cc in range(2):
-        for b in range(vb):
-            at = (cc * vb + b) * LANES
-            for i in range(2):
-                lhs[i * n_kv : (i + 1) * n_kv, at : at + LANES] = headsf[
-                    pl.ds(cc * hrows + i * (hrows // 2) + b, n_kv, stride=2 * hrows), :
-                ].astype(BF16)
+    for b in range(vb):
+        for i in range(2):
+            lhs[i * n_kv : (i + 1) * n_kv, b * LANES : (b + 1) * LANES] = headsf[
+                pl.ds(i * (hrows // 2) + b, n_kv, stride=hrows), :
+            ].astype(BF16)
     remote(wo.at[other], wo.at[other], psem.at[2], psem.at[3], kv, other).wait_recv()
-    projected = dot(lhs[...], wo[...].reshape(LANES, 2 * vb * LANES), ((1,), (1,)))
+    own_rows = pl.ds(pl.multiple_of(c * vb * LANES, LANES), vb * LANES)
+    partial[0] = dot(lhs[...], wo[:, :, own_rows].reshape(LANES, vb * LANES), ((1,), (1,)))
+    send(partial.at[0], partial.at[1], psem.at[4], psem.at[5], kv, other)
+    remote(partial.at[1], partial.at[1], psem.at[4], psem.at[5], kv, other).wait_recv()
+    projected = partial[0] + partial[1]
+    after = [
+        (tokf[pl.ds(i, n_kv, stride=2), :] + projected[i * n_kv : (i + 1) * n_kv]).astype(BF16)
+        for i in range(2)
+    ]
     for i in range(2):
-        old = tokf[pl.ds(i, n_kv, stride=2), :]
-        whole[2 * kv + i] = (old + projected[i * n_kv : (i + 1) * n_kv]).astype(BF16)
+        kept[i] = after[i].astype(F32)
+    whole[kv] = jnp.where(c == 0, after[0].astype(F32), after[1].astype(F32)).astype(BF16)
 
     mark("gather_after")
-    in_mlp[0].wait()
-    in_mlp[1].wait()
-    sums = [
-        jnp.zeros((2 * n_kv, LANES), F32),
-        jnp.zeros(hidden.shape, F32),
-        jnp.zeros(hidden.shape, F32),
-    ]
+    remote(wm.at[other], wm.at[other], psem.at[6], psem.at[7], kv, other).wait_recv()
+    units = hidden.shape[2]
+    energy = [jnp.zeros((n_kv, LANES), F32)]
+    sums = [jnp.zeros((n_kv, units), F32) for _ in range(4)]
 
     def multiply(zp):
         parts = []
         for xp in range(NX):
             k = zp * NX + xp
-            rows = jnp.concatenate([whole[2 * k], whole[2 * k + 1]], axis=0).astype(F32)
-            sums[0] = sums[0] + rows * rows
+            rows = whole[k].astype(F32)
+            energy[0] = energy[0] + rows * rows
             parts.append((rows * mgainf[pl.ds(k, 1), :]).astype(BF16))
         rows = jnp.concatenate(parts, axis=1)
         cols = pl.ds(pl.multiple_of(zp * NX * LANES, LANES), NX * LANES)
-        sums[1] = sums[1] + dot(rows, wmg[:, cols], ((1,), (1,)))
-        sums[2] = sums[2] + dot(rows, wmu[:, cols], ((1,), (1,)))
-
-    gather(whole, asem, False, multiply)
+        for k in range(4):
+            sums[k] = sums[k] + dot(rows, wm[k // 2, k % 2, :, cols], ((1,), (1,)))
+
+    gather(whole, asem, multiply)
 
     mark("mlp_in")
-    inv = lax.rsqrt(jnp.sum(sums[0], axis=1, keepdims=True) * (1.0 / width) + EPS)
-    gate = sums[1] * inv
-    up = sums[2] * inv
-    hidden[...] = (gate / (1.0 + jnp.exp(-gate)) * up).astype(BF16)
+    inv = lax.rsqrt(jnp.sum(energy[0], axis=1, keepdims=True) * (1.0 / width) + EPS)
+    for cc in range(2):
+        gate = sums[2 * cc] * inv
+        up = sums[2 * cc + 1] * inv
+        hidden[cc] = (gate / (1.0 + jnp.exp(-gate)) * up).astype(BF16)
     mark("mlp_down")
-    in_mlp[2].wait()
     for g in range(2):
         for j in range(nh):
             cols = pl.ds(pl.multiple_of(zrel(g, j) * NX * LANES, LANES), NX * LANES)
-            part = dot(hidden[...], wmd[:, cols]).astype(BF16)
+            part = (dot(hidden[0], wm[0, 2, :, cols]) + dot(hidden[1], wm[1, 2, :, cols])).astype(
+                BF16
+            )
             for xp in range(NX):
-                for k in range(4):
-                    dpart[k // 2, g, 2 * xp + k % 2, :, j * LANES : (j + 1) * LANES] = part[
+                for k in range(2):
+                    dx[g, 2 * xp + k, :, j * LANES : (j + 1) * LANES] = part[
                         k * n_kv // 2 : (k + 1) * n_kv // 2, xp * LANES : (xp + 1) * LANES
                     ]
-        send(dpart.at[other, g], dpeer.at[g], psem.at[4], psem.at[5 + g], kv, other)
-    mark("down_peer")
-
-    for g in range(2):
-        remote(dpeer.at[g], dpeer.at[g], psem.at[4], psem.at[5 + g], kv, other).wait_recv()
-        for n, xp in enumerate(sides + [x]):
-            for k in range(2):
-                dx[g, 2 * xp + k] = (
-                    dpart[c, g, 2 * xp + k].astype(F32) + dpeer[g, 2 * xp + k].astype(F32)
-                ).astype(BF16)
-            if n < NX - 1:
-                send(
-                    dx.at[g, pl.ds(2 * xp, 2)],
-                    drb.at[g, pl.ds(2 * n, 2)],
-                    dxsem.at[g, 0],
-                    dxsem.at[g, 1],
-                    z * NX + xp,
-                    c,
-                )
+        for n, xp in enumerate(sides):
+            send(
+                dx.at[g, pl.ds(2 * xp, 2)],
+                drb.at[g, pl.ds(2 * n, 2)],
+                dxsem.at[g, 0],
+                dxsem.at[g, 1],
+                z * NX + xp,
+                c,
+            )
     low_lanes = lax.broadcasted_iota(jnp.int32, (n_kv // 2, LANES), 1) < LANES // 2
 
     def squeeze(top, bottom, right):
@@ -657,7 +626,7 @@
     remote(part, part, dzsem.at[0], dzsem.at[1], kv, other).wait_recv()
     mark("finish")
     for i in range(2):
-        rows = whole[2 * kv + i].astype(F32)
+        rows = kept[i]
         halves = rows[: n_kv // 2], rows[n_kv // 2 :]
         total = jnp.where(c == 1, squeeze(*halves, True), squeeze(*halves, False))
         for zp in range(nz):
@@ -676,9 +645,10 @@
             remote(part, part, zsem.at[stage, 0], zsem.at[stage, 1], left, c).wait_send()
         part = drb.at[g]
         remote(part, part, dxsem.at[g, 0], dxsem.at[g, 1], left, c).wait_send()
-    gather_drain(headb, hsem, True)
-    gather_drain(whole, asem, False)
-    remote(dpeer, dpeer, psem.at[4], psem.at[5], kv, other).wait_send()
+    gather_drain(headb, hsem)
+    gather_drain(whole, asem)
+    remote(partial.at[0], partial.at[1], psem.at[4], psem.at[5], kv, other).wait_send()
+    remote(wm.at[c], wm.at[c], psem.at[6], psem.at[7], kv, other).wait_send()
     part = dzr.at[pl.ds(0, 2 * nz - 1)]
     remote(part, part, dzsem.at[0], dzsem.at[1], kv, other).wait_send()
     mark()
@@ -731,9 +701,7 @@
         vmem(cache_values.shape, bf),
         vmem(cache_rates.shape, fl),
         vmem((2,) + w_out.shape[::-1], bf),
-        vmem(w_mlp_gate.shape[::-1], bf),
-        vmem(w_mlp_up.shape[::-1], bf),
-        vmem(w_mlp_down.shape, bf),
+        vmem((2, 3) + w_mlp_down.shape, bf),
         vmem((2, NX * 2, nz, half0 * LANES), bf),
         vmem((2, NX * 2, nz, half1 * LANES), bf),
         vmem((2, 2, nz, half0 * LANES), bf),
@@ -752,13 +720,13 @@
         vmem((2 * vb, LANES), fl),
         vmem((vb, LANES), fl),
         vmem((hrows, LANES), fl),
-        vmem((2 * n_kv, hrows, LANES), bf),
-        vmem((n_kv * 2 * hrows, LANES), fl),
-        vmem((seqs, 2 * vb * LANES), bf),
-        vmem((2 * n_kv, n_kv, LANES), bf),
-        vmem((seqs, units), bf),
-        vmem((2, 2, NX * 2, n_kv // 2, cols5), bf),
-        vmem((2, NX * 2, n_kv // 2, cols5), bf),
+        vmem((n_kv, hrows, LANES), bf),
+        vmem((n_kv * hrows, LANES), fl),
+        vmem((seqs, vb * LANES), bf),
+        vmem((n_kv, n_kv, LANES), bf),
+        vmem((2, n_kv, units), bf),
+        vmem((2, seqs, LANES), fl),
+        vmem((2, n_kv, LANES), fl),
         vmem((2, NX * 2, n_kv // 2, cols5), bf),
         vmem((2, 2 * (NX - 1), n_kv // 2, cols5), bf),
         vmem((2 * nz, n_kv // 2, LANES), bf),
@@ -769,12 +737,12 @@
         vmem((n_kv, LANES), bf),
         vmem((n_kv, LANES), fl),
         pltpu.SMEM((2,), jnp.int32),
-        dma((18,)),
-        dma((7,)),
+        dma((16,)),
+        dma((8,)),
         dma((4, 4)),
         dma((4, 2)),
-        dma((1 + 3 * nz,)),
-        dma((1 + 3 * nz,)),
+        dma((1 + 2 * nz,)),
+        dma((1 + 2 * nz,)),
         dma((2, 2)),
         dma((2,)),
         pltpu.SemaphoreType.REGULAR((max(1, 2 * (nz // 2) - 3),)),
@@ -784,7 +752,7 @@
     specs = [anywhere] * 18
     return pl.pallas_call(
         functools.partial(kernel, (nz, qb, vb, dk, width)),
-        out_shape=jax.ShapeDtypeStruct(tokens.shape, BF16),
+        out_shape=pltpu.VMEM(tokens.shape, BF16),
         in_specs=specs,
         out_specs=in_vmem,
         scratch_shapes=scratch,

time: 56.6 us -> 51.2 us (0.905)
  Pallas kernels: 55 us -> 50.5 us
  local copies, waits for them, and re-layouts: 1.32 us -> 0.61 us
    pallas_call x1, Pallas kernels: 55 us -> 50.5 us  [shards(): pl.pallas_call(functools.partial(kernel, (nz, qb, vb, dk, width)), out_sh...]
    unnamed x1, local copies, waits for them, and re-layouts: 1.32 us -> 0.61 us
where the time goes in v7:
time: 51.2 us; the launch traced here: 51.1 us
  Pallas kernels  50.5 us (99%)
  local copies, waits for them, and re-layouts  0.61 us (1%)
    pallas_call x1, Pallas kernels, shards(): pl.pallas_call(functools.partial(kernel, (nz, qb, vb, dk, width)), out_sh...  50.5 us

profile of v7, /device:TPU:1, one launch (start us, length us, event | category | flops | bytes accessed | tf_op | source)
XLA Modules:
  0.0 51.1 jit_solution(5274388064384403602)
XLA Ops:
  0.0 50.5 %layer.1 = bf16[64,64]{1,0:T(8,128)(2,1)S(1)} custom-call(bf16[64,64]{1,0:T(8,128)(2,1)} %tokens.1, s32[2]{0:T(128)} %lengths.1, f32[2,2,384,768]{3,2,1,0:T(8,128)} %state.1, bf16[2,2,64,384]{3,2,1,0:T(8,128)(2,1)} %cache_keys.1, bf16[2,2,64,768]{3,2,1,0:T(8,128)(2,1)} %cache_values.1, f32[2,2,64,384]{3,2,1,0:T(8,128)} %cache_rates.1, ...), custom_call_target="tpu_custom_call" | custom-call | tf_op jit(solution)/shard_map/layer/pallas_call | solution.py:753
  50.5 0.6 %copy.20 = bf16[64,64]{1,0:T(8,128)(2,1)} copy(bf16[64,64]{1,0:T(8,128)(2,1)S(1)} %layer.1) | data formatting | bytes 16384

commit v8 on v7

--- a/solution.py
+++ b/solution.py
@@ -77,12 +77,12 @@
     att,
     hg,
     headf,
+    hmine,
     headb,
     headsf,
     lhs,
     whole,
     hidden,
-    partial,
     kept,
     dx,
     drb,
@@ -372,11 +372,12 @@
     x_second(*x_stage(1, 0))
     x_second(*x_stage(1, 1))
 
-    slots_row = zf.shape[0] // (2 * nh)
+    slots_of = (pack0.shape[0] // 2, pack1.shape[0] // 2)
 
     def z_send(g, col):
         src, first, relay, back, stage = x_stage(g, col)
         half = src.shape[2] // LANES
+        slots_row = slots_of[col]
         x_wait(back, stage)
         for hh in (0, 1):
             total = x_sum(src, back, hh)
@@ -386,11 +387,11 @@
                         i * nh : (i + 1) * nh, b * LANES : (b + 1) * LANES
                     ]
         for j in by_distance(g):
-            zs[stage, j] = zf[j * 2 * slots_row : (j + 1) * 2 * slots_row, :].astype(BF16)
+            zs[stage, j, : 2 * slots_row] = zf[j * 2 * slots_row : (j + 1) * 2 * slots_row, :].astype(BF16)
             if (g, j) != (self_g, self_j):
                 send(
-                    zs.at[stage, j],
-                    zr.at[stage, j],
+                    zs.at[stage, j, pl.ds(0, 2 * slots_row)],
+                    zr.at[stage, j, pl.ds(0, 2 * slots_row)],
                     zsem.at[stage, 0],
                     zsem.at[stage, 1],
                     zrel(g, j) * NX + x,
@@ -398,18 +399,19 @@
                 )
 
     def z_part(g, col):
-        return zr.at[2 * g + col, pl.ds(0, nh - (g == self_g))]
+        return zr.at[2 * g + col, pl.ds(0, nh - (g == self_g)), pl.ds(0, 2 * slots_of[col])]
 
     def z_sum(col):
         for g in range(2):
             part = z_part(g, col)
             stage = 2 * g + col
             remote(part, part, zsem.at[stage, 0], zsem.at[stage, 1], left, c).wait_recv()
-        total = zs[2 * self_g + col, self_j].astype(F32)
+        rows = slice(0, 2 * slots_of[col])
+        total = zs[2 * self_g + col, self_j, rows].astype(F32)
         for g in range(2):
             for j in range(nh):
                 if (g, j) != (self_g, self_j):
-                    total = total + zr[2 * g + col, j].astype(F32)
+                    total = total + zr[2 * g + col, j, rows].astype(F32)
         return total
 
     chain_wait(2)
@@ -434,7 +436,7 @@
     inverse = []
     qh = qb // 2
     for i in range(2):
-        at = i * slots_row
+        at = i * slots_of[0]
         inv = lax.rsqrt(pack0[at + 3 * qb : at + 3 * qb + 1, :] * (1.0 / width) + EPS)
         inverse.append(inv)
         query = pack0[at : at + qb, :] * inv * dk ** (-0.5)
@@ -461,7 +463,7 @@
     mark("z_wait_b")
     pack1[...] = z_sum(1)
     for i in range(2):
-        at = i * slots_row
+        at = i * slots_of[1]
         if i == 0:
             mark("heads_b")
         value = pack1[at : at + vb, :] * inverse[i]
@@ -476,7 +478,10 @@
             headf[i * (headf.shape[0] // 2) + h * hb : i * (headf.shape[0] // 2) + (h + 1) * hb, :] = (
                 g / (1.0 + jnp.exp(-g)) * norm
             )
-    headb[kv] = headf[...].astype(BF16)
+    mrows = headf.shape[0] // 2
+    for i in range(2):
+        hmine[i] = headf[i * mrows : (i + 1) * mrows, :].astype(BF16)
+    headb[2 * kv + c] = jnp.where(c == 0, headf[:mrows, :], headf[mrows:, :]).astype(BF16)
 
     def gather(buf, sems, consume):
         out_sem = sems.at[0]
@@ -508,35 +513,43 @@
         remote(part, part, sems.at[0], sems.at[1], left, c).wait_send()
 
     n_kv = nz * NX
-    hrows = headf.shape[0]
-
-    def widen(zp):
-        for k in range(NX):
-            slot = NX * zp + k
-            headsf[pl.ds(pl.multiple_of(slot * hrows, 8), hrows), :] = headb[slot].astype(F32)
 
     mark("gather_heads")
-    gather(headb, hsem, widen)
+    out_sem = hsem.at[0]
+    slot = headb.at[2 * kv + c]
+    for zp in far:
+        send(hmine.at[c], slot, out_sem, hsem.at[1 + z], zp * NX + x, c)
+        send(hmine.at[other], slot, out_sem, hsem.at[1 + z], zp * NX + x, other)
+    send(hmine.at[other], slot, out_sem, hsem.at[1 + z], kv, other)
+    for zp in [z] + near:
+        part = headb.at[pl.ds(0, 2 - (zp is z))]
+        remote(part, part, out_sem, hsem.at[1 + zp], zp * NX + x, other).wait_recv()
+        pair = headb.at[pl.ds(2 * (zp * NX + x), 2)]
+        for xp in sides:
+            send(pair, pair, out_sem, hsem.at[1 + nz + zp], z * NX + xp, c)
+    mark("heads_x")
+    for zp in [z] + near:
+        part = headb.at[pl.ds(0, 2 * (NX - 1))]
+        remote(part, part, out_sem, hsem.at[1 + nz + zp], left, c).wait_recv()
+        for k in range(2 * NX):
+            at = 2 * NX * zp + k
+            headsf[pl.ds(pl.multiple_of(at * mrows, 8), mrows), :] = headb[at].astype(F32)
 
     mark("project_out")
-    for b in range(vb):
-        for i in range(2):
-            lhs[i * n_kv : (i + 1) * n_kv, b * LANES : (b + 1) * LANES] = headsf[
-                pl.ds(i * (hrows // 2) + b, n_kv, stride=hrows), :
+    for cc in range(2):
+        for b in range(vb):
+            at = (cc * vb + b) * LANES
+            lhs[:, at : at + LANES] = headsf[
+                pl.ds(cc * mrows + b, n_kv, stride=2 * mrows), :
             ].astype(BF16)
     remote(wo.at[other], wo.at[other], psem.at[2], psem.at[3], kv, other).wait_recv()
-    own_rows = pl.ds(pl.multiple_of(c * vb * LANES, LANES), vb * LANES)
-    partial[0] = dot(lhs[...], wo[:, :, own_rows].reshape(LANES, vb * LANES), ((1,), (1,)))
-    send(partial.at[0], partial.at[1], psem.at[4], psem.at[5], kv, other)
-    remote(partial.at[1], partial.at[1], psem.at[4], psem.at[5], kv, other).wait_recv()
-    projected = partial[0] + partial[1]
-    after = [
-        (tokf[pl.ds(i, n_kv, stride=2), :] + projected[i * n_kv : (i + 1) * n_kv]).astype(BF16)
-        for i in range(2)
-    ]
-    for i in range(2):
-        kept[i] = after[i].astype(F32)
-    whole[kv] = jnp.where(c == 0, after[0].astype(F32), after[1].astype(F32)).astype(BF16)
+    projected = dot(lhs[...], wo[...].reshape(LANES, 2 * vb * LANES), ((1,), (1,)))
+    tokens_half = jnp.where(
+        c == 0, tokf[pl.ds(0, n_kv, stride=2), :], tokf[pl.ds(1, n_kv, stride=2), :]
+    )
+    after = (tokens_half + projected).astype(BF16)
+    whole[kv] = after
+    kept[c] = after
 
     mark("gather_after")
     remote(wm.at[other], wm.at[other], psem.at[6], psem.at[7], kv, other).wait_recv()
@@ -557,6 +570,7 @@
             sums[k] = sums[k] + dot(rows, wm[k // 2, k % 2, :, cols], ((1,), (1,)))
 
     gather(whole, asem, multiply)
+    send(kept.at[c], kept.at[c], psem.at[4], psem.at[5], kv, other)
 
     mark("mlp_in")
     inv = lax.rsqrt(jnp.sum(energy[0], axis=1, keepdims=True) * (1.0 / width) + EPS)
@@ -625,15 +639,16 @@
     part = dzr.at[pl.ds(0, 2 * nz - 1)]
     remote(part, part, dzsem.at[0], dzsem.at[1], kv, other).wait_recv()
     mark("finish")
+    remote(kept.at[other], kept.at[other], psem.at[4], psem.at[5], kv, other).wait_recv()
     for i in range(2):
-        rows = kept[i]
+        rows = kept[i].astype(F32)
         halves = rows[: n_kv // 2], rows[n_kv // 2 :]
         total = jnp.where(c == 1, squeeze(*halves, True), squeeze(*halves, False))
         for zp in range(nz):
             total = total + dzr[2 * zp + i].astype(F32)
         outf[pl.ds(i, n_kv // 2, stride=2), :] = total
         outf[pl.ds(i + n_kv, n_kv // 2, stride=2), :] = pltpu.roll(total, LANES // 2, 1)
-    out[...] = outf[:, : LANES // 2].astype(BF16)
+    out[...] = outf[:, : LANES // 2]
     mark("drain")
     remote(tok.at[c], tok.at[c], psem.at[0], psem.at[1], kv, other).wait_send()
     remote(wo.at[c], wo.at[c], psem.at[2], psem.at[3], kv, other).wait_send()
@@ -645,9 +660,10 @@
             remote(part, part, zsem.at[stage, 0], zsem.at[stage, 1], left, c).wait_send()
         part = drb.at[g]
         remote(part, part, dxsem.at[g, 0], dxsem.at[g, 1], left, c).wait_send()
-    gather_drain(headb, hsem)
+    part = headb.at[pl.ds(0, 2 * nz * NX - 1)]
+    remote(part, part, hsem.at[0], hsem.at[1], left, c).wait_send()
     gather_drain(whole, asem)
-    remote(partial.at[0], partial.at[1], psem.at[4], psem.at[5], kv, other).wait_send()
+    remote(kept.at[c], kept.at[c], psem.at[4], psem.at[5], kv, other).wait_send()
     remote(wm.at[c], wm.at[c], psem.at[6], psem.at[7], kv, other).wait_send()
     part = dzr.at[pl.ds(0, 2 * nz - 1)]
     remote(part, part, dzsem.at[0], dzsem.at[1], kv, other).wait_send()
@@ -680,10 +696,11 @@
     width = mlp_gain.shape[0]
     qb, vb = heads * dk // LANES, heads * dv // LANES
     half0, half1 = (3 * qb + 2) // 2, vb
-    slots = -(-2 * max(half0, half1) // 8) * 8
+    slots_a, slots_b = [-(-2 * half // 4) * 4 for half in (half0, half1)]
+    slots = max(slots_a, slots_b)
     nh = nz // 2
     seqs = 2 * n_kv
-    hrows = 2 * vb
+    mrows = -(-vb // 8) * 8
     units = w_mlp_down.shape[0]
     cols5 = nh * LANES
     vmem, dma = pltpu.VMEM, pltpu.SemaphoreType.DMA
@@ -714,19 +731,19 @@
         vmem((4, nh, 2 * slots, LANES), bf),
         vmem((4, nh, 2 * slots, LANES), bf),
         vmem(state.shape, bf),
-        vmem((2 * slots, LANES), fl),
-        vmem((2 * slots, LANES), fl),
+        vmem((2 * slots_a, LANES), fl),
+        vmem((2 * slots_b, LANES), fl),
         vmem((2 * qb, LANES), fl),
         vmem((2 * vb, LANES), fl),
         vmem((vb, LANES), fl),
-        vmem((hrows, LANES), fl),
-        vmem((n_kv, hrows, LANES), bf),
-        vmem((n_kv * hrows, LANES), fl),
-        vmem((seqs, vb * LANES), bf),
+        vmem((2 * mrows, LANES), fl),
+        vmem((2, mrows, LANES), bf),
+        vmem((2 * n_kv, mrows, LANES), bf),
+        vmem((2 * n_kv * mrows, LANES), fl),
+        vmem((n_kv, 2 * vb * LANES), bf),
         vmem((n_kv, n_kv, LANES), bf),
         vmem((2, n_kv, units), bf),
-        vmem((2, seqs, LANES), fl),
-        vmem((2, n_kv, LANES), fl),
+        vmem((2, n_kv, LANES), bf),
         vmem((2, NX * 2, n_kv // 2, cols5), bf),
         vmem((2, 2 * (NX - 1), n_kv // 2, cols5), bf),
         vmem((2 * nz, n_kv // 2, LANES), bf),
@@ -750,9 +767,9 @@
     anywhere = pl.BlockSpec(memory_space=pl.ANY)
     in_vmem = pl.BlockSpec(memory_space=pltpu.VMEM)
     specs = [anywhere] * 18
-    return pl.pallas_call(
+    summed = pl.pallas_call(
         functools.partial(kernel, (nz, qb, vb, dk, width)),
-        out_shape=pltpu.VMEM(tokens.shape, BF16),
+        out_shape=pltpu.VMEM(tokens.shape, F32),
         in_specs=specs,
         out_specs=in_vmem,
         scratch_shapes=scratch,
@@ -778,6 +795,7 @@
         w_mlp_up.T,
         w_mlp_down,
     )
+    return summed.astype(BF16)
 
 
 def solution(mesh):

time: 51.2 us -> 50.8 us (level)
  other arithmetic: 0 us -> 0.61 us
  local copies, waits for them, and re-layouts: 0.61 us -> 0 us
    convert_element_type x0 -> x1, other arithmetic: none -> 0.61 us  [shards(): return summed.astype(BF16)]
    unnamed x1 -> x0, local copies, waits for them, and re-layouts: 0.61 us -> none
where the time goes in v8:
time: 50.8 us; the launch traced here: 50.7 us
  Pallas kernels  50.1 us (99%)
  other arithmetic  0.61 us (1%)
    pallas_call x1, Pallas kernels, shards(): pl.pallas_call(functools.partial(kernel, (nz, qb, vb, dk, width)), out_sh...  50.1 us

profile of v8, /device:TPU:1, one launch (start us, length us, event | category | flops | bytes accessed | tf_op | source)
XLA Modules:
  0.0 50.7 jit_solution(17654047653194556647)
XLA Ops:
  0.0 50.1 %layer.1 = f32[64,64]{1,0:T(8,128)S(1)} custom-call(bf16[64,64]{1,0:T(8,128)(2,1)} %tokens.1, s32[2]{0:T(128)} %lengths.1, f32[2,2,384,768]{3,2,1,0:T(8,128)} %state.1, bf16[2,2,64,384]{3,2,1,0:T(8,128)(2,1)} %cache_keys.1, bf16[2,2,64,768]{3,2,1,0:T(8,128)(2,1)} %cache_values.1, f32[2,2,64,384]{3,2,1,0:T(8,128)} %cache_rates.1, bf16[1,128]{1,0:T(2,128)(2,1)} %bitcast.9, ...), custom_call_target="tpu_custom_call" | custom-call | tf_op jit(solution)/shard_map/layer/pallas_call | solution.py:770
  50.1 0.6 %convert_element_type.3 = bf16[64,64]{1,0:T(8,128)(2,1)} convert(f32[64,64]{1,0:T(8,128)S(1)} %layer.1) | non-fusion elementwise | flops 4096 | bytes 24576 | tf_op jit(solution)/shard_map/convert_element_type | solution.py:798

commit v9 on v8

--- a/solution.py
+++ b/solution.py
@@ -727,7 +727,7 @@
         vmem((2, 2, nz, half1 * LANES), bf),
         vmem((2, 4, nz, half0 * LANES), bf),
         vmem((2, 4, nz, half1 * LANES), bf),
-        vmem((nz * slots, LANES), fl),
+        vmem((2 * nz * slots, LANES), fl),
         vmem((4, nh, 2 * slots, LANES), bf),
         vmem((4, nh, 2 * slots, LANES), bf),
         vmem(state.shape, bf),

time: 50.8 us -> 50.8 us (level)
  no operation moved by 1% of the time
where the time goes in v9:
time: 50.8 us; the launch traced here: 50.7 us
  Pallas kernels  50.1 us (99%)
  other arithmetic  0.61 us (1%)
    pallas_call x1, Pallas kernels, shards(): pl.pallas_call(functools.partial(kernel, (nz, qb, vb, dk, width)), out_sh...  50.1 us

profile of v9, /device:TPU:1, one launch (start us, length us, event | category | flops | bytes accessed | tf_op | source)
XLA Modules:
  0.0 50.7 jit_solution(7351038226220813843)
XLA Ops:
  0.0 50.1 %layer.1 = f32[64,64]{1,0:T(8,128)S(1)} custom-call(bf16[64,64]{1,0:T(8,128)(2,1)} %tokens.1, s32[2]{0:T(128)} %lengths.1, f32[2,2,384,768]{3,2,1,0:T(8,128)} %state.1, bf16[2,2,64,384]{3,2,1,0:T(8,128)(2,1)} %cache_keys.1, bf16[2,2,64,768]{3,2,1,0:T(8,128)(2,1)} %cache_values.1, f32[2,2,64,384]{3,2,1,0:T(8,128)} %cache_rates.1, bf16[1,128]{1,0:T(2,128)(2,1)} %bitcast.9, ...), custom_call_target="tpu_custom_call" | custom-call | tf_op jit(solution)/shard_map/layer/pallas_call | solution.py:770
  50.1 0.6 %convert_element_type.3 = bf16[64,64]{1,0:T(8,128)(2,1)} convert(f32[64,64]{1,0:T(8,128)S(1)} %layer.1) | non-fusion elementwise | flops 4096 | bytes 24576 | tf_op jit(solution)/shard_map/convert_element_type | solution.py:798
